TPU v7x, 256 devices: a whole 4x4x8 slice. The times are simulated.
256 devices in a mesh: sp: 64 (over z, y, core), tp: 4 (over x).
Axes of the slice: x: 4, y: 4, z: 8, core: 2. Of those that a mesh axis runs over, the one named last changes fastest.
Arguments:
- resid: bfloat16 [12288, 2048], P('sp'), may hold values from -6 to 6
- query_broad: bfloat16 [12288, 1536], P('sp', 'tp'), may hold values from -60 to 60
- query_narrow: bfloat16 [12288, 1024], P('sp', 'tp'), may hold values from -60 to 60
- latent: bfloat16 [12288, 512], P('sp'), may hold values from -6 to 6
- key_rope: bfloat16 [12288, 64], P('sp'), may hold values from -6 to 6
- latent_gain: float32 [512], replicated, may hold values from 0.1 to 1.9
- key_up_broad: bfloat16 [512, 1024], P(None, 'tp'), may hold values from -0.25 to 0.25
- value_up_broad: bfloat16 [512, 1024], P(None, 'tp'), may hold values from -0.25 to 0.25
- key_up_narrow: bfloat16 [512, 512], P(None, 'tp'), may hold values from -0.25 to 0.25
- value_up_narrow: bfloat16 [512, 512], P(None, 'tp'), may hold values from -0.25 to 0.25
- out_broad: bfloat16 [1024, 2048], replicated, may hold values from -0.15625 to 0.15625
- out_narrow: bfloat16 [512, 2048], replicated, may hold values from -0.15625 to 0.15625
- post_gain: float32 [2048], replicated, may hold values from 0.1 to 1.9
- ffn_gain: float32 [2048], replicated, may hold values from 0.1 to 1.9
- up_weight: bfloat16 [2048, 8192], P('sp', 'tp'), may hold values from -0.125 to 0.125
- down_weight: bfloat16 [2048, 8192], P('sp', 'tp'), may hold values from -0.0625 to 0.0625
- ffn_out_gain: float32 [2048], replicated, may hold values from 0.1 to 1.9
Outputs:
- layer_out: bfloat16 [12288, 2048], P(('sp', 'tp'))
All inputs are finite; a program needn't handle non-finite values.
Results may differ from a plain program's by a relative error of at most 0.013.
Values may be sent and summed in bfloat16 or wider, within the bound.
A program may use at most 128 MiB of HBM per device.

v0:
```python
import math

import jax
import jax.numpy as jnp
from jax import lax
from jax.sharding import PartitionSpec as P

DB = 128
DN = 64


norm_eps = 1e-06
rope_base = 500000.0
masked_score = -1e30


def sent_together(arrays, axis, dim, along):
    ends, at = ([], 0)
    for a in arrays[:-1]:
        at += a.shape[along]
        ends.append(at)
    both = jnp.concatenate(arrays, axis=along)
    return tuple(jnp.split(lax.all_gather(both, axis, axis=dim, tiled=True), ends, axis=along))


def split_up(value, dim, size):
    before, after = (value.shape[:dim], value.shape[dim + 1 :])
    return jnp.moveaxis(value.reshape(*before, size, -1, *after), dim, 0)


def sum_at_owner(value, axis, dim):
    size = lax.axis_size(axis)
    parts = lax.all_to_all(split_up(value, dim, size), axis, 0, 0, tiled=True)
    return jnp.sum(parts.astype(jnp.float32), axis=0)


def rotate(values, positions):
    full_width = values.shape[-1]
    half_width = full_width // 2
    frequency = rope_base ** (-2.0 * jnp.arange(half_width, dtype=jnp.float32) / full_width)
    angles = positions.astype(jnp.float32)[:, None] * frequency[None, :]
    angle_shape = (angles.shape[0],) + (1,) * (values.ndim - 2) + (half_width,)
    cosine = jnp.cos(angles).reshape(angle_shape)
    sine_part = jnp.sin(angles).reshape(angle_shape)
    leading = values[..., :half_width]
    trailing = values[..., half_width:]
    return jnp.concatenate(
        [leading * cosine - trailing * sine_part, trailing * cosine + leading * sine_part], axis=-1
    )


def rms_scale(values, norm_gain):
    return (
        values * lax.rsqrt(jnp.mean(values * values, axis=-1, keepdims=True) + norm_eps) * norm_gain
    )


def group_update(
    running, nope_query, rope_query, key_rows, key_rot, value_rows, score_scale, allowed
):
    old_max, old_sum, old_acc = running
    scores = jnp.einsum("qhd,khd->hqk", nope_query, key_rows, preferred_element_type=jnp.float32)
    scores = scores + jnp.einsum(
        "qhd,kd->hqk", rope_query, key_rot, preferred_element_type=jnp.float32
    )
    scores = jnp.where(allowed, scores * score_scale, masked_score)
    new_max = jnp.maximum(old_max, jnp.max(scores, axis=-1))
    exponent = jnp.where(allowed, jnp.exp(scores - new_max[:, :, None]), 0.0)
    factor = jnp.exp(old_max - new_max)
    new_sum = old_sum * factor + jnp.sum(exponent, axis=-1)
    weighted = jnp.einsum(
        "hqk,khd->qhd",
        exponent.astype(jnp.bfloat16),
        value_rows,
        preferred_element_type=jnp.float32,
    )
    new_acc = old_acc * jnp.transpose(factor)[:, :, None] + weighted
    return (new_max, new_sum, new_acc)


def local(
    resid,
    query_broad,
    query_narrow,
    latent,
    key_rope,
    latent_gain,
    key_up_broad,
    value_up_broad,
    key_up_narrow,
    value_up_narrow,
    out_broad,
    out_narrow,
    post_gain,
    ffn_gain,
    up_weight,
    down_weight,
    ffn_out_gain,
):
    local_rows = resid.shape[0]
    head_parts = lax.axis_size("tp")
    share_rows = local_rows // head_parts
    row_offset = lax.axis_index("sp") * local_rows
    last_query = row_offset + local_rows - 1
    query_pos = row_offset + jnp.arange(local_rows, dtype=jnp.int32)
    rope_width = key_rope.shape[1]
    broad_count = key_up_broad.shape[1] // DB
    narrow_count = key_up_narrow.shape[1] // DN
    broad_heads = query_broad.reshape(local_rows, broad_count, DB + rope_width)
    broad_nope = broad_heads[:, :, :DB]
    broad_rope = rotate(broad_heads[:, :, DB:].astype(jnp.float32), query_pos).astype(jnp.bfloat16)
    narrow_heads = query_narrow.reshape(local_rows, narrow_count, DN + rope_width)
    narrow_nope = narrow_heads[:, :, :DN]
    narrow_rope = rotate(narrow_heads[:, :, DN:].astype(jnp.float32), query_pos).astype(
        jnp.bfloat16
    )
    broad_scale = (DB + rope_width) ** (-0.5)
    narrow_scale = (DN + rope_width) ** (-0.5)

    def attend(running, latent_rows, rope_rows, first_row):
        key_count = latent_rows.shape[0]
        key_pos = first_row + jnp.arange(key_count, dtype=jnp.int32)
        latent_normed = rms_scale(latent_rows.astype(jnp.float32), latent_gain).astype(jnp.bfloat16)

        def expand(weight, head_size):
            product = jnp.dot(latent_normed, weight, preferred_element_type=jnp.float32)
            return product.astype(jnp.bfloat16).reshape(key_count, -1, head_size)

        key_rot = rotate(rope_rows.astype(jnp.float32), key_pos).astype(jnp.bfloat16)
        allowed = (key_pos[None, :] <= query_pos[:, None])[None]
        broad_state = group_update(
            running[0],
            broad_nope,
            broad_rope,
            expand(key_up_broad, DB),
            key_rot,
            expand(value_up_broad, DB),
            broad_scale,
            allowed,
        )
        narrow_state = group_update(
            running[1],
            narrow_nope,
            narrow_rope,
            expand(key_up_narrow, DN),
            key_rot,
            expand(value_up_narrow, DN),
            narrow_scale,
            allowed,
        )
        return (broad_state, narrow_state)

    def fresh(head_count, head_size):
        return (
            jnp.full((head_count, local_rows), masked_score, jnp.float32),
            jnp.zeros((head_count, local_rows), jnp.float32),
            jnp.zeros((local_rows, head_count, head_size), jnp.float32),
        )

    initial = (fresh(broad_count, DB), fresh(narrow_count, DN))
    latent_piece, rope_piece = sent_together((latent, key_rope), "sp", 0, 1)
    piece_rows = latent_piece.shape[0]
    block_rows = math.gcd(piece_rows, 1024)

    def one_block(block_index, carried):
        begin = block_index * block_rows
        latent_block = lax.dynamic_slice_in_dim(latent_piece, begin, block_rows, 0)
        rope_block = lax.dynamic_slice_in_dim(rope_piece, begin, block_rows, 0)

        def unchanged(kept_state):
            return kept_state

        def updated(kept_state):
            return attend(kept_state, latent_block, rope_block, begin)

        return lax.cond(begin > last_query, unchanged, updated, carried)

    final_state = lax.fori_loop(0, piece_rows // block_rows, one_block, initial)

    def finish(running):
        run_max, run_sum, run_acc = running
        return (
            (run_acc / jnp.transpose(run_sum)[:, :, None])
            .astype(jnp.bfloat16)
            .reshape(local_rows, -1)
        )

    attn_broad = finish(final_state[0])
    attn_narrow = finish(final_state[1])
    rows_broad, rows_narrow = (
        lax.all_to_all(attn_broad, "tp", split_axis=0, concat_axis=1, tiled=True),
        lax.all_to_all(attn_narrow, "tp", split_axis=0, concat_axis=1, tiled=True),
    )
    projected = jnp.dot(rows_broad, out_broad, preferred_element_type=jnp.float32) + jnp.dot(
        rows_narrow, out_narrow, preferred_element_type=jnp.float32
    )
    own_resid = lax.dynamic_slice_in_dim(resid, lax.axis_index("tp") * share_rows, share_rows, 0)
    mixed = (own_resid.astype(jnp.float32) + rms_scale(projected, post_gain)).astype(jnp.bfloat16)
    normed = rms_scale(mixed.astype(jnp.float32), ffn_gain).astype(jnp.bfloat16)
    up_full, down_full = sent_together((up_weight, down_weight), "sp", 0, 1)
    hidden = jnp.square(
        jax.nn.relu(
            jnp.dot(
                lax.all_gather(normed, "tp", axis=0, tiled=True),
                up_full,
                preferred_element_type=jnp.float32,
            )
        )
    ).astype(jnp.bfloat16)
    ffn = sum_at_owner(
        lax.dot_general(
            hidden, down_full, (((1,), (1,)), ((), ())), preferred_element_type=jnp.float32
        ).astype(jnp.bfloat16),
        "tp",
        0,
    )
    return (mixed.astype(jnp.float32) + rms_scale(ffn, ffn_out_gain)).astype(jnp.bfloat16)


def solution(mesh):
    in_specs = (
        P("sp", None),
        P("sp", "tp"),
        P("sp", "tp"),
        P("sp", None),
        P("sp", None),
        P(),
        P(None, "tp"),
        P(None, "tp"),
        P(None, "tp"),
        P(None, "tp"),
        P(),
        P(),
        P(),
        P(),
        P("sp", "tp"),
        P("sp", "tp"),
        P(),
    )
    out_specs = P(("sp", "tp"), None)
    return jax.shard_map(local, mesh=mesh, in_specs=in_specs, out_specs=out_specs, check_vma=False)
```

profile of v0, /device:TPU:232, one launch (start us, length us, event | category | flops | bytes accessed | tf_op | source)
XLA Modules:
  0.0 369.3 jit_solution(1359104549341646893)
XLA Ops:
  11.8 92.0 %all-gather.3.cloned.1.call-done = bf16[12288,576]{1,0:T(8,128)(2,1)} async-done(((bf16[192,576]{1,0:T(8,128)(2,1)}), bf16[12288,576]{1,0:T(8,128)(2,1)}) %all-gather.3.cloned.1.call-update) | async-done | bytes 14155792 | tf_op jit(solution)/shard_map/all_gather | solution.py:23
  103.8 3.2 split.17
  106.9 4.3 %copy.42 = bf16[12288,64]{0,1:T(8,128)(2,1)} copy(bf16[12288,64]{1,0:T(8,128)(2,1)} %split.17) | data formatting | bytes 3145728
  111.2 10.5 %split.16 = bf16[12288,512]{1,0:T(8,128)(2,1)} slice(bf16[12288,576]{1,0:T(8,128)(2,1)} %all-gather.3.cloned.1.call-done), slice={[0:12288], [0:512]} | slice | bytes 25165824 | tf_op jit(solution)/shard_map/split | solution.py:23
  121.9 180.2 %while.24 = (s32[]{:T(128)}, f32[2,192]{1,0:T(2,128)S(1)}, f32[2,192]{1,0:T(2,128)S(1)}, f32[192,2,128]{2,0,1:T(8,128)S(1)}, f32[2,192]{1,0:T(2,128)S(1)}, /*ind...) while((s32[]{:T(128)}, f32[2,192]{1,0:T(2,128)S(1)}, ...), condition=%wide.region_8.9_spmd.clone, body=%wide.region_0.8_spmd.clone.sunk | while | flops 1227806208 | bytes 28073760 | solution.py:178
  121.9 15.0 %conditional.3 = (f32[2,192]{1,0:T(2,128)S(1)}, f32[2,192]{1,0:T(2,128)S(1)}, f32[192,2,128]{2,0,1:T(8,128)S(1)}, f32[2,192]{1,0:T(2,128)S(1)}, f32[2,192]{1,0:T(2,128)S(1)}, /*index=5*/f32[192,2,64]{0,2,1:T(8,128)S(1)}) conditional(s32[]{:T(128)} %convert_element_type.191, (s32[]{:T(128)}, s32[]{:T(128)}, bf16[12288,512]{1,0:T(8,128)(2,1)}, ...), branch_computations={%region_1.6_spmd, %region_7.7_spmd} | conditional | flops 1227806208 | bytes 28066418 | solution.py:176
  134.4 1.9 convolution_convert_fusion
  137.0 14.9 %conditional.3 = (f32[2,192]{1,0:T(2,128)S(1)}, f32[2,192]{1,0:T(2,128)S(1)}, f32[192,2,128]{2,0,1:T(8,128)S(1)}, f32[2,192]{1,0:T(2,128)S(1)}, f32[2,192]{1,0:T(2,128)S(1)}, /*index=5*/f32[192,2,64]{0,2,1:T(8,128)S(1)}) conditional(s32[]{:T(128)} %convert_element_type.191, (s32[]{:T(128)}, s32[]{:T(128)}, bf16[12288,512]{1,0:T(8,128)(2,1)}, ...), branch_computations={%region_1.6_spmd, %region_7.7_spmd} | conditional | flops 1227806208 | bytes 28066418 | solution.py:176
  151.9 15.0 %conditional.3 = (f32[2,192]{1,0:T(2,128)S(1)}, f32[2,192]{1,0:T(2,128)S(1)}, f32[192,2,128]{2,0,1:T(8,128)S(1)}, f32[2,192]{1,0:T(2,128)S(1)}, f32[2,192]{1,0:T(2,128)S(1)}, /*index=5*/f32[192,2,64]{0,2,1:T(8,128)S(1)}) conditional(s32[]{:T(128)} %convert_element_type.191, (s32[]{:T(128)}, s32[]{:T(128)}, bf16[12288,512]{1,0:T(8,128)(2,1)}, ...), branch_computations={%region_1.6_spmd, %region_7.7_spmd} | conditional | flops 1227806208 | bytes 28066418 | solution.py:176
  164.3 1.9 convolution_convert_fusion
  166.9 15.1 %conditional.3 = (f32[2,192]{1,0:T(2,128)S(1)}, f32[2,192]{1,0:T(2,128)S(1)}, f32[192,2,128]{2,0,1:T(8,128)S(1)}, f32[2,192]{1,0:T(2,128)S(1)}, f32[2,192]{1,0:T(2,128)S(1)}, /*index=5*/f32[192,2,64]{0,2,1:T(8,128)S(1)}) conditional(s32[]{:T(128)} %convert_element_type.191, (s32[]{:T(128)}, s32[]{:T(128)}, bf16[12288,512]{1,0:T(8,128)(2,1)}, ...), branch_computations={%region_1.6_spmd, %region_7.7_spmd} | conditional | flops 1227806208 | bytes 28066418 | solution.py:176
  168.5 1.9 convolution_convert_fusion.3
  175.6 2.0 convolution_convert_fusion.1
  179.5 1.9 convolution_convert_fusion
  182.1 15.2 %conditional.3 = (f32[2,192]{1,0:T(2,128)S(1)}, f32[2,192]{1,0:T(2,128)S(1)}, f32[192,2,128]{2,0,1:T(8,128)S(1)}, f32[2,192]{1,0:T(2,128)S(1)}, f32[2,192]{1,0:T(2,128)S(1)}, /*index=5*/f32[192,2,64]{0,2,1:T(8,128)S(1)}) conditional(s32[]{:T(128)} %convert_element_type.191, (s32[]{:T(128)}, s32[]{:T(128)}, bf16[12288,512]{1,0:T(8,128)(2,1)}, ...), branch_computations={%region_1.6_spmd, %region_7.7_spmd} | conditional | flops 1227806208 | bytes 28066418 | solution.py:176
  188.4 1.9 convolution_convert_fusion.2
  194.7 1.9 convolution_convert_fusion
  197.3 14.9 %conditional.3 = (f32[2,192]{1,0:T(2,128)S(1)}, f32[2,192]{1,0:T(2,128)S(1)}, f32[192,2,128]{2,0,1:T(8,128)S(1)}, f32[2,192]{1,0:T(2,128)S(1)}, f32[2,192]{1,0:T(2,128)S(1)}, /*index=5*/f32[192,2,64]{0,2,1:T(8,128)S(1)}) conditional(s32[]{:T(128)} %convert_element_type.191, (s32[]{:T(128)}, s32[]{:T(128)}, bf16[12288,512]{1,0:T(8,128)(2,1)}, ...), branch_computations={%region_1.6_spmd, %region_7.7_spmd} | conditional | flops 1227806208 | bytes 28066418 | solution.py:176
  212.3 14.9 %conditional.3 = (f32[2,192]{1,0:T(2,128)S(1)}, f32[2,192]{1,0:T(2,128)S(1)}, f32[192,2,128]{2,0,1:T(8,128)S(1)}, f32[2,192]{1,0:T(2,128)S(1)}, f32[2,192]{1,0:T(2,128)S(1)}, /*index=5*/f32[192,2,64]{0,2,1:T(8,128)S(1)}) conditional(s32[]{:T(128)} %convert_element_type.191, (s32[]{:T(128)}, s32[]{:T(128)}, bf16[12288,512]{1,0:T(8,128)(2,1)}, ...), branch_computations={%region_1.6_spmd, %region_7.7_spmd} | conditional | flops 1227806208 | bytes 28066418 | solution.py:176
  227.3 14.9 %conditional.3 = (f32[2,192]{1,0:T(2,128)S(1)}, f32[2,192]{1,0:T(2,128)S(1)}, f32[192,2,128]{2,0,1:T(8,128)S(1)}, f32[2,192]{1,0:T(2,128)S(1)}, f32[2,192]{1,0:T(2,128)S(1)}, /*index=5*/f32[192,2,64]{0,2,1:T(8,128)S(1)}) conditional(s32[]{:T(128)} %convert_element_type.191, (s32[]{:T(128)}, s32[]{:T(128)}, bf16[12288,512]{1,0:T(8,128)(2,1)}, ...), branch_computations={%region_1.6_spmd, %region_7.7_spmd} | conditional | flops 1227806208 | bytes 28066418 | solution.py:176
  242.3 14.9 %conditional.3 = (f32[2,192]{1,0:T(2,128)S(1)}, f32[2,192]{1,0:T(2,128)S(1)}, f32[192,2,128]{2,0,1:T(8,128)S(1)}, f32[2,192]{1,0:T(2,128)S(1)}, f32[2,192]{1,0:T(2,128)S(1)}, /*index=5*/f32[192,2,64]{0,2,1:T(8,128)S(1)}) conditional(s32[]{:T(128)} %convert_element_type.191, (s32[]{:T(128)}, s32[]{:T(128)}, bf16[12288,512]{1,0:T(8,128)(2,1)}, ...), branch_computations={%region_1.6_spmd, %region_7.7_spmd} | conditional | flops 1227806208 | bytes 28066418 | solution.py:176
  257.2 14.9 %conditional.3 = (f32[2,192]{1,0:T(2,128)S(1)}, f32[2,192]{1,0:T(2,128)S(1)}, f32[192,2,128]{2,0,1:T(8,128)S(1)}, f32[2,192]{1,0:T(2,128)S(1)}, f32[2,192]{1,0:T(2,128)S(1)}, /*index=5*/f32[192,2,64]{0,2,1:T(8,128)S(1)}) conditional(s32[]{:T(128)} %convert_element_type.191, (s32[]{:T(128)}, s32[]{:T(128)}, bf16[12288,512]{1,0:T(8,128)(2,1)}, ...), branch_computations={%region_1.6_spmd, %region_7.7_spmd} | conditional | flops 1227806208 | bytes 28066418 | solution.py:176
  272.2 14.9 %conditional.3 = (f32[2,192]{1,0:T(2,128)S(1)}, f32[2,192]{1,0:T(2,128)S(1)}, f32[192,2,128]{2,0,1:T(8,128)S(1)}, f32[2,192]{1,0:T(2,128)S(1)}, f32[2,192]{1,0:T(2,128)S(1)}, /*index=5*/f32[192,2,64]{0,2,1:T(8,128)S(1)}) conditional(s32[]{:T(128)} %convert_element_type.191, (s32[]{:T(128)}, s32[]{:T(128)}, bf16[12288,512]{1,0:T(8,128)(2,1)}, ...), branch_computations={%region_1.6_spmd, %region_7.7_spmd} | conditional | flops 1227806208 | bytes 28066418 | solution.py:176
  287.1 14.9 %conditional.3 = (f32[2,192]{1,0:T(2,128)S(1)}, f32[2,192]{1,0:T(2,128)S(1)}, f32[192,2,128]{2,0,1:T(8,128)S(1)}, f32[2,192]{1,0:T(2,128)S(1)}, f32[2,192]{1,0:T(2,128)S(1)}, /*index=5*/f32[192,2,64]{0,2,1:T(8,128)S(1)}) conditional(s32[]{:T(128)} %convert_element_type.191, (s32[]{:T(128)}, s32[]{:T(128)}, bf16[12288,512]{1,0:T(8,128)(2,1)}, ...), branch_computations={%region_1.6_spmd, %region_7.7_spmd} | conditional | flops 1227806208 | bytes 28066418 | solution.py:176
  303.0 4.3 %all-to-all-start = ((bf16[4,48,256]{2,1,0:T(8,128)(2,1)}), bf16[4,48,256]{2,1,0:T(8,128)(2,1)S(1)}, u32[]{:S(2)}, u32[]{:S(2)}) async-start(bf16[4,48,256]{2,1,0:T(8,128)(2,1)} %all_to_all.31), calls=%async_computation | async-start | bytes 196608 | tf_op jit(solution)/shard_map/all_to_all | solution.py:191
  308.2 4.9 %all-to-all-done = bf16[4,48,256]{2,1,0:T(8,128)(2,1)S(1)} async-done(((bf16[4,48,256]{2,1,0:T(8,128)(2,1)}), bf16[4,48,256]{2,1,0:T(8,128)(2,1)S(1)}, u32[]{:S(2)}, u32[]{:S(2)}) %all-to-all-start) | async-done | bytes 98336 | tf_op jit(solution)/shard_map/all_to_all | solution.py:191
  313.1 3.3 all-to-all-start.1
  316.4 3.0 fusion.72
  319.5 2.4 all-to-all-done.1
  323.8 14.9 %all_gather.10 = bf16[192,2048]{1,0:T(8,128)(2,1)} all-gather(bf16[48,2048]{1,0:T(8,128)(2,1)S(1)} %fusion.64), channel_id=1, replica_groups=mesh['sp'=64,'tp'=4] {'tp'}, dimensions={0}, use_global_device_ids=true | all-gather | bytes 983040 | tf_op jit(solution)/shard_map/all_gather | solution.py:204
  338.7 10.6 %fusion.53 = bf16[192,2048]{1,0:T(8,128)(2,1)S(1)} fusion(bf16[2048,4096]{1,0:T(8,128)(2,1)} %all-gather.5.cloned.1.call-done, bf16[192,2048]{1,0:T(8,128)(2,1)} %all_gather.10), kind=kOutput, calls=%fused_computation.67 | convolution fusion | flops 3222798336 | bytes 18350080 | tf_op jit(solution)/shard_map/dot_general | solution.py:211
  349.3 12.1 %all_to_all.43 = bf16[4,48,2048]{2,1,0:T(8,128)(2,1)S(1)} all-to-all(bf16[4,48,2048]{2,1,0:T(8,128)(2,1)S(1)} %bitcast.74), channel_id=1, replica_groups=mesh['sp'=64,'tp'=4] {'tp'}, dimensions={0} | all-to-all | bytes 1572864 | tf_op jit(solution)/shard_map/all_to_all | solution.py:33
  (368 shorter events, 174.4 us)
Async XLA Ops:
  6.5 315.4 %copy-start = (bf16[512,2048]{1,0:T(8,128)(2,1)S(1)}, bf16[512,2048]{1,0:T(8,128)(2,1)}, u32[]{:S(2)}) copy-start(bf16[512,2048]{1,0:T(8,128)(2,1)} %param.32) | copy-start | bytes 6291460
  6.5 4.5 %copy-start.2 = (bf16[192,256]{1,0:T(8,128)(2,1)S(1)}, bf16[192,256]{1,0:T(8,128)(2,1)}, u32[]{:S(2)}) copy-start(bf16[192,256]{1,0:T(8,128)(2,1)} %param.23) | copy-start | bytes 294916
  6.5 4.6 %copy-start.1 = (bf16[192,384]{1,0:T(8,128)(2,1)S(1)}, bf16[192,384]{1,0:T(8,128)(2,1)}, u32[]{:S(2)}) copy-start(bf16[192,384]{1,0:T(8,128)(2,1)} %param.22) | copy-start | bytes 442372
  6.5 97.2 %all-gather.3.cloned.1.call-start = ((), (), s32[]{:S(2)}) async-start(), calls=%async_computation.3 | async-start | bytes 15974400 | tf_op jit(solution)/shard_map/all_gather | solution.py:23
  9.3 329.5 %all-gather.5.cloned.1.call-start = ((), (), s32[]{:S(2)}) async-start(), calls=%async_computation.4 | async-start | bytes 17039360 | tf_op jit(solution)/shard_map/all_gather | solution.py:23
  111.2 10.6 %copy-start.6 = (bf16[512,256]{1,0:T(8,128)(2,1)S(1)}, bf16[512,256]{1,0:T(8,128)(2,1)}, u32[]{:S(2)}) copy-start(bf16[512,256]{1,0:T(8,128)(2,1)} %param.27) | copy-start | bytes 786436
  111.2 10.6 %copy-start.7 = (bf16[512,256]{1,0:T(8,128)(2,1)S(1)}, bf16[512,256]{1,0:T(8,128)(2,1)}, u32[]{:S(2)}) copy-start(bf16[512,256]{1,0:T(8,128)(2,1)} %param.28) | copy-start | bytes 786436
  111.2 10.6 %copy-start.8 = (bf16[512,128]{1,0:T(8,128)(2,1)S(1)}, bf16[512,128]{1,0:T(8,128)(2,1)}, u32[]{:S(2)}) copy-start(bf16[512,128]{1,0:T(8,128)(2,1)} %param.29) | copy-start | bytes 393220
  111.2 10.6 %copy-start.9 = (bf16[512,128]{1,0:T(8,128)(2,1)S(1)}, bf16[512,128]{1,0:T(8,128)(2,1)}, u32[]{:S(2)}) copy-start(bf16[512,128]{1,0:T(8,128)(2,1)} %param.30) | copy-start | bytes 393220
  111.2 10.6 %copy-start.10 = (f32[512]{0:T(512)S(1)}, f32[512]{0:T(512)}, u32[]{:S(2)}) copy-start(f32[512]{0:T(512)} %param.26) | copy-start | bytes 6148
  303.0 10.1 %all-to-all-start = ((bf16[4,48,256]{2,1,0:T(8,128)(2,1)}), bf16[4,48,256]{2,1,0:T(8,128)(2,1)S(1)}, u32[]{:S(2)}, u32[]{:S(2)}) async-start(bf16[4,48,256]{2,1,0:T(8,128)(2,1)} %all_to_all.31), calls=%async_computation | async-start | bytes 196608 | tf_op jit(solution)/shard_map/all_to_all | solution.py:191
  313.1 8.8 %all-to-all-start.1 = ((bf16[4,48,128]{2,1,0:T(8,128)(2,1)}), bf16[4,48,128]{2,1,0:T(8,128)(2,1)S(1)}, u32[]{:S(2)}, u32[]{:S(2)}) async-start(bf16[4,48,128]{2,1,0:T(8,128)(2,1)} %all_to_all.35), calls=%async_computation.1 | async-start | bytes 98304 | tf_op jit(solution)/shard_map/all_to_all | solution.py:192
  319.5 3.1 copy-start.3
  319.5 4.3 %copy-start.5 = (f32[2048]{0:T(1024)S(1)}, f32[2048]{0:T(1024)}, u32[]{:S(2)}) copy-start(f32[2048]{0:T(1024)} %param.34) | copy-start | bytes 24580
  349.3 12.4 %copy-start.4 = (f32[2048]{0:T(1024)S(1)}, f32[2048]{0:T(1024)}, u32[]{:S(2)}) copy-start(f32[2048]{0:T(1024)} %param.37) | copy-start | bytes 24580
Sparse Core Ops, SparseCore 0:
  10.1 93.6 all-gather.2
  106.5 96.2 all-gather.4
where the time goes:
time: 373 us; the launch traced here: 369 us
  matrix products  142 us (38%)
  waiting for transfers between devices  99.4 us (27%)
  other arithmetic  55.9 us (15%)
  blocking collectives  27 us (7%)
  local copies, waits for them, and re-layouts  21.2 us (6%)
  between operations  13.7 us (4%)
  starting transfers between devices  7.6 us (2%)
    all_gather x2, waiting for transfers between devices, sent_together(): lax.all_gather(both, axis, axis=dim, tiled=True)  92 us
    dot_general x48, matrix products, expand(): product = jnp.dot(latent_normed, weight, preferred_element_type=jnp.float32)  90.3 us
    reduce_sum x14, other arithmetic, rms_scale(): jnp.mean(values * values, axis=-1, keepdims=True) + norm_eps  19.5 us
    all_gather x1, blocking collectives, local(): lax.all_gather(normed, 'tp', axis=0, tiled=True)  14.9 us
    split x2, local copies, waits for them, and re-layouts, sent_together(): jnp.split(lax.all_gather(both, axis, axis=dim, tiled=True), ends, axis=al...  13.7 us
    dot_general x24, matrix products, group_update(): jnp.einsum('hqk,khd->qhd', exponent.astype(jnp.bfloat16), value_rows, pre...  13.4 us
    dot_general x24, matrix products, group_update(): jnp.einsum('qhd,kd->hqk', rope_query, key_rot, preferred_element_type=jnp...  12.6 us
    all_to_all x1, blocking collectives, sum_at_owner(): parts = lax.all_to_all(split_up(value, dim, size), axis, 0, 0, tiled=True)  12.1 us
  transfers between devices with their start and end apart: 4, of which 3 were waited for; matrix products, arithmetic and copies ran while one was open for 55% of the time, Pallas kernels for 0%

commit v1 on v0

v1 whole, which is shorter than its diff:
```python
import functools
import math

import jax
import jax.numpy as jnp
from jax import lax
from jax.experimental import pallas as pl
from jax.experimental.pallas import tpu as pltpu
from jax.sharding import PartitionSpec as P

DB = 128
DN = 64
ROPE = 64
NY = 4

norm_eps = 1e-06
rope_base = 500000.0
broad_unit = (DB + ROPE) ** (-0.5) * math.log2(math.e)
narrow_unit = (DN + ROPE) ** (-0.5) * math.log2(math.e)
f32 = jnp.float32
bf16 = jnp.bfloat16


def dot(a, b, dims=((1,), (0,))):
    return lax.dot_general(a, b, (dims, ((), ())), preferred_element_type=f32)


def picker(shape, pick):
    rows = lax.broadcasted_iota(jnp.int32, shape, 0)
    columns = lax.broadcasted_iota(jnp.int32, shape, 1)
    return jnp.where(pick(rows, columns), 1.0, 0.0).astype(bf16)


LAST = ((1,), (1,))


def prepare(core, q_broad, q_narrow, cosines, sines, refs, qt_broad, qt_narrow, w_key, w_value_t):
    key_up_broad, value_up_broad, key_up_narrow, value_up_narrow = refs
    at = core * (DB + ROPE)
    rows = q_broad.shape[0]
    wide = q_broad.shape[1]
    qt_broad[0:DB] = dot(
        picker((DB, wide), lambda r, k: k == r + at), q_broad, LAST
    ).astype(bf16)
    qt_broad[DB : DB + 64] = jnp.zeros((64, rows), bf16)

    def rotated(value, start):
        straight = dot(picker((64, value.shape[1]), lambda r, k: k == r + start), value, LAST)
        swapped = dot(
            picker(
                (64, value.shape[1]), lambda r, k: k == jnp.where(r < 32, r + 32, r - 32) + start
            ),
            value,
            LAST,
        )
        return (straight * cosines + swapped * sines).astype(bf16)

    qt_broad[DB + 64 : DB + 128] = rotated(q_broad, at + DB)
    at_n = core * (DN + ROPE)
    qt_narrow[0:64] = dot(
        picker((64, q_narrow.shape[1]), lambda r, k: k == r + at_n), q_narrow, LAST
    ).astype(bf16)
    qt_narrow[64:128] = rotated(q_narrow, at_n + DN)
    w_key[:, 0:DB] = key_up_broad[:, pl.ds(pl.multiple_of(core * DB, DB), DB)]
    w_key[:, DB : DB + 128] = dot(
        key_up_narrow[...], picker((128, 128), lambda r, k: (r == k + core * DN) & (k < DN))
    ).astype(bf16)
    w_value_t[0:DB] = dot(
        picker((DB, 2 * DB), lambda r, k: k == r + core * DB), value_up_broad[...], LAST
    ).astype(bf16)
    w_value_t[DB : DB + DN] = dot(
        picker((DN, 2 * DN), lambda r, k: k == r + core * DN), value_up_narrow[...], LAST
    ).astype(bf16)


def attend_block(block, diagonal, qt_broad, qt_narrow, w_key, w_value_t, top, total, acc):
    keys, queries = block.shape[0], qt_broad.shape[1]
    latent = block[:, 0:512]
    expanded = dot(latent, w_key[...])
    key_b = expanded[:, 0:DB].astype(bf16)
    key_n = (expanded[:, DB : DB + 128] + block[:, 512:640].astype(f32)).astype(bf16)
    value_t = dot(w_value_t[...], latent, LAST).astype(bf16)
    score_b = dot(jnp.concatenate([key_b, key_n], axis=1), qt_broad[...])
    score_n = dot(key_n, qt_narrow[...])
    if diagonal:
        allowed = lax.broadcasted_iota(jnp.int32, (keys, queries), 0) <= lax.broadcasted_iota(
            jnp.int32, (keys, queries), 1
        )
    for head, (score, unit, start, size) in enumerate(
        ((score_b, broad_unit, 0, DB), (score_n, narrow_unit, DB, DN))
    ):
        if diagonal:
            score = jnp.where(allowed, score, -1e30)
            peak = jnp.max(score, axis=0, keepdims=True)
        else:
            peak = jnp.maximum(top[head], jnp.max(score, axis=0, keepdims=True))
        weight = jnp.exp2((score - peak) * unit)
        if diagonal:
            weight = jnp.where(allowed, weight, 0.0)
        added = jnp.sum(weight, axis=0, keepdims=True)
        product = dot(value_t[start : start + size], weight.astype(bf16))
        if diagonal:
            total[head] = added
            acc[start : start + size] = product
        else:
            factor = jnp.exp2((top[head] - peak) * unit)
            total[head] = total[head] * factor + added
            acc[start : start + size] = acc[start : start + size] * factor + product
        top[head] = peak


def ring_places(axis_size):
    return lambda at, step: lax.rem(at + step + axis_size, axis_size)


class Spread:
    def __init__(self, held, sent, arrived, place, first, first_cut, rest_cut):
        self.held, self.sent, self.arrived = held, sent, arrived
        self.z, self.y, self.core = place
        self.nz, self.ny, _, self.rows, _ = held.shape
        self.first, self.first_cut, self.rest_cut = first, first_cut, rest_cut
        self.half_z, self.half_y = self.nz // 2, self.ny // 2
        names = [("ay", s, d) for s in (0, 1) for d in (1, -1)]
        for s in range(self.half_z):
            for d in (1, -1):
                names.append(("bz", s, d))
                for ch in (0, 1):
                    if s < self.half_z - 1 or ch == (0 if d == 1 else 1):
                        names.append(("az", s, d, ch))
                        names.append(("pa", s, d, ch))
        for s in (0, 1):
            for d in (1, -1):
                for ch in (0, 1):
                    if s == 0 or ch == (0 if d == 1 else 1):
                        names.append(("by", s, d, ch))
                        names.append(("pb", s, d, ch))
        names += [("pa", -1, 1, 0), ("pa", -1, 1, 1), ("pb", -1, 1, 0)]
        self.index = {name: i for i, name in enumerate(names)}

    @staticmethod
    def count(nz, ny):
        return 4 + (nz // 2) * 2 + 2 * ((nz // 2 - 1) * 4 + 2) + 2 * 6 + 3

    def device(self, z, y, core):
        return {"sp": (z * self.ny + y) * 2 + core}

    def copy(self, name):
        kind, s, d = name[:3]
        zs, ys = ring_places(self.nz), ring_places(self.ny)
        z, y, c, held, first = self.z, self.y, self.core, self.held, self.first
        low, high = pl.ds(0, first), pl.ds(first, self.rows - first)
        i = self.index[name]
        if kind == "ay":
            if s == 1:
                low = (
                    pl.ds(0, self.first_cut)
                    if d == 1
                    else pl.ds(self.first_cut, first - self.first_cut)
                )
            view, to = held.at[z, ys(y, -s * d), c, low], self.device(z, ys(y, d), c)
        elif kind == "bz":
            if s == self.half_z - 1:
                high = (
                    pl.ds(first, self.rest_cut)
                    if d == 1
                    else pl.ds(first + self.rest_cut, self.rows - first - self.rest_cut)
                )
            view, to = held.at[zs(z, -s * d), y, c, high], self.device(zs(z, d), y, c)
        elif kind == "az":
            part = pl.ds(name[3] * self.half_y, self.half_y)
            view, to = held.at[zs(z, -s * d), part, c, low], self.device(zs(z, d), y, c)
        elif kind == "by":
            part = pl.ds(name[3] * self.half_z, self.half_z)
            view, to = held.at[part, ys(y, -s * d), c, high], self.device(z, ys(y, d), c)
        elif kind == "pa":
            part = pl.ds(name[3] * self.half_y, self.half_y)
            view, to = held.at[zs(z, -(s + 1) * d), part, c, low], self.device(z, y, 1 - c)
        else:
            part = pl.ds(0, self.nz) if s == -1 else pl.ds(name[3] * self.half_z, self.half_z)
            view, to = held.at[part, ys(y, -(s + 1) * d), c, high], self.device(z, y, 1 - c)
        return pltpu.make_async_remote_copy(
            src_ref=view,
            dst_ref=view,
            send_sem=self.sent.at[i],
            recv_sem=self.arrived.at[i],
            device_id=to,
            device_id_type=pl.DeviceIdType.MESH,
        )

    def start(self, *names):
        for name in names:
            self.copy(name).start()

    def landed(self, *names):
        for name in names:
            self.copy(name).wait_recv()

    def both(self, kind, s):
        return [n for n in self.index if n[0] == kind and n[1] == s]

    def begin(self):
        self.start(*self.both("ay", 0), *self.both("bz", 0))

    def open_rings(self):
        self.landed(*self.both("ay", 0))
        self.start(*self.both("ay", 1))
        self.landed(*self.both("bz", 0))
        self.start(*self.both("bz", 1))
        self.landed(*self.both("ay", 1))
        self.start(*self.both("az", 0), *self.both("pa", -1))
        for s in range(1, self.half_z):
            self.landed(*self.both("bz", s))
            if s + 1 < self.half_z:
                self.start(*self.both("bz", s + 1))
        self.start(*self.both("by", 0), *self.both("pb", -1))

    def pass_on(self, name):
        kind, s, d, ch = name
        self.landed(name)
        following = (kind, s + 1, d, ch)
        if following in self.index:
            self.start(following)
        self.start(("p" + kind[0], s, d, ch))

    def order(self):
        names = []
        for s in range(self.half_z):
            if s == self.half_z // 2:
                names += self.both("by", 0)
            if s == self.half_z - 1:
                names += self.both("by", 1)
            names += self.both("az", s)
        return names

    def own_chip(self):
        return [*self.both("pa", -1), *self.both("pb", -1)]

    def handed(self):
        return [n for n in self.index if n[0] in ("pa", "pb") and n[1] >= 0]

    def drain(self):
        for name in self.index:
            self.copy(name).wait_send()


def attention_kernel(
    geometry,
    rows_hbm,
    q_broad,
    q_narrow,
    cosines,
    sines,
    key_up_broad,
    value_up_broad,
    key_up_narrow,
    value_up_narrow,
    out,
    held,
    all_q_broad,
    all_q_narrow,
    qt_broad,
    qt_narrow,
    w_key,
    w_value_t,
    top,
    total,
    acc,
    finished,
    own_sem,
    sent,
    arrived,
    more_sent,
    more_arrived,
):
    nz, ny, first, first_cut, rest_cut = geometry
    me = lax.axis_index("sp")
    core = lax.rem(me, 2)
    chip = me // 2
    z, y = chip // ny, lax.rem(chip, ny)
    rows = rows_hbm.shape[0]
    zs, ys = ring_places(nz), ring_places(ny)
    spread = Spread(held, sent, arrived, (z, y, core), first, first_cut, rest_cut)

    own = pltpu.make_async_copy(rows_hbm, held.at[z, y, core], own_sem)
    own.start()
    barrier = pltpu.get_barrier_semaphore()
    neighbours = [
        spread.device(z, y, 1 - core),
        spread.device(z, ys(y, 1), core),
        spread.device(z, ys(y, -1), core),
        spread.device(zs(z, 1), y, core),
        spread.device(zs(z, -1), y, core),
    ]
    for neighbour in neighbours:
        pl.semaphore_signal(
            barrier, inc=1, device_id=neighbour, device_id_type=pl.DeviceIdType.MESH
        )
    pl.semaphore_wait(barrier, len(neighbours))
    own.wait()
    spread.begin()

    def to_partner(src, dst, i):
        return pltpu.make_async_remote_copy(
            src_ref=src,
            dst_ref=dst,
            send_sem=more_sent.at[i],
            recv_sem=more_arrived.at[i],
            device_id=spread.device(z, y, 1 - core),
            device_id_type=pl.DeviceIdType.MESH,
        )

    exchange = [
        to_partner(q_broad, all_q_broad.at[core], 0),
        to_partner(q_narrow, all_q_narrow.at[core], 1),
    ]
    for copy in exchange:
        copy.start()
    all_q_broad[core] = q_broad[...]
    all_q_narrow[core] = q_narrow[...]
    spread.open_rings()
    for copy in exchange:
        copy.wait_recv()
    prepare(
        core,
        all_q_broad[...].reshape(2 * rows, -1),
        all_q_narrow[...].reshape(2 * rows, -1),
        cosines[...],
        sines[...],
        (key_up_broad, value_up_broad, key_up_narrow, value_up_narrow),
        qt_broad,
        qt_narrow,
        w_key,
        w_value_t,
    )
    spread.landed(*spread.own_chip())
    tools = (qt_broad, qt_narrow, w_key, w_value_t, top, total, acc)

    def block_of(k):
        return held[k // ny, lax.rem(k, ny)].reshape(2 * rows, -1)

    attend_block(block_of(chip), True, *tools)
    for name in spread.order():
        spread.pass_on(name)
    spread.landed(*spread.handed())

    def earlier(k, carried):
        attend_block(block_of(k), False, *tools)
        return carried

    lax.fori_loop(0, chip, earlier, 0)
    broad = jnp.transpose(acc[0:DB] / total[0])
    narrow = jnp.transpose(acc[DB : DB + DN] / total[1])
    finished[...] = (
        jnp.concatenate([broad, narrow], axis=1).astype(bf16).reshape(2, rows, DB + DN)
    )
    result = to_partner(finished.at[1 - core], out.at[core], 2)
    result.start()
    out[core] = finished[core]
    spread.drain()
    for copy in exchange:
        copy.wait_send()
    result.wait()


def attention(geometry, packed, q_broad, q_narrow, cosines, sines, ups):
    nz, ny = geometry[:2]
    rows, width = packed.shape
    vmem = pl.BlockSpec(memory_space=pltpu.VMEM)
    copies = Spread.count(nz, ny)
    return pl.pallas_call(
        functools.partial(attention_kernel, geometry),
        out_shape=jax.ShapeDtypeStruct((2, rows, DB + DN), bf16),
        in_specs=[pl.BlockSpec(memory_space=pl.ANY)] + [vmem] * 8,
        out_specs=vmem,
        scratch_shapes=[
            pltpu.VMEM((nz, ny, 2, rows, width), bf16),
            pltpu.VMEM((2, rows, q_broad.shape[1]), bf16),
            pltpu.VMEM((2, rows, q_narrow.shape[1]), bf16),
            pltpu.VMEM((256, 2 * rows), bf16),
            pltpu.VMEM((128, 2 * rows), bf16),
            pltpu.VMEM((512, 256), bf16),
            pltpu.VMEM((DB + DN, 512), bf16),
            pltpu.VMEM((2, 1, 2 * rows), f32),
            pltpu.VMEM((2, 1, 2 * rows), f32),
            pltpu.VMEM((DB + DN, 2 * rows), f32),
            pltpu.VMEM((2, rows, DB + DN), bf16),
            pltpu.SemaphoreType.DMA,
            pltpu.SemaphoreType.DMA((copies,)),
            pltpu.SemaphoreType.DMA((copies,)),
            pltpu.SemaphoreType.DMA((3,)),
            pltpu.SemaphoreType.DMA((3,)),
        ],
        compiler_params=pltpu.CompilerParams(
            collective_id=0, has_side_effects=True, vmem_limit_bytes=56 * 1024 * 1024
        ),
        cost_estimate=pl.CostEstimate(
            flops=40_000_000_000, bytes_accessed=20_000_000, transcendentals=9_000_000
        ),
        name="attention",
    )(packed, q_broad, q_narrow, cosines, sines, *ups)


def rms_scale(values, norm_gain):
    return (
        values * lax.rsqrt(jnp.mean(values * values, axis=-1, keepdims=True) + norm_eps) * norm_gain
    )


def angles_of(first, count):
    frequency = rope_base ** (-2.0 * jnp.arange(ROPE // 2, dtype=f32) / ROPE)
    positions = (first + jnp.arange(count, dtype=jnp.int32)).astype(f32)
    return positions, frequency


def local(
    resid,
    query_broad,
    query_narrow,
    latent,
    key_rope,
    latent_gain,
    key_up_broad,
    value_up_broad,
    key_up_narrow,
    value_up_narrow,
    out_broad,
    out_narrow,
    post_gain,
    ffn_gain,
    up_weight,
    down_weight,
    ffn_out_gain,
):
    rows = resid.shape[0]
    parts = lax.axis_size("tp")
    share = rows // parts
    me = lax.axis_index("sp")
    ny = NY
    nz = lax.axis_size("sp") // (2 * ny)

    positions, frequency = angles_of(me * rows, rows)
    angles = positions[:, None] * frequency[None, :]
    cosine, sine = jnp.cos(angles), jnp.sin(angles)
    leading, trailing = jnp.split(key_rope.astype(f32), 2, axis=1)
    latent_normed = rms_scale(latent.astype(f32), latent_gain).astype(bf16)
    packed = jnp.concatenate(
        [
            latent_normed,
            jnp.zeros((rows, 64), bf16),
            (leading * cosine - trailing * sine).astype(bf16),
            (trailing * cosine + leading * sine).astype(bf16),
        ],
        axis=1,
    )
    positions, frequency = angles_of((me // 2) * 2 * rows, 2 * rows)
    angles = frequency[:, None] * positions[None, :]
    cosine, sine = jnp.cos(angles), jnp.sin(angles)
    cosines = jnp.concatenate([cosine, cosine], axis=0)
    sines = jnp.concatenate([-sine, sine], axis=0)
    geometry = (nz, ny, 80, 48, 64)
    attn = attention(
        geometry,
        packed,
        query_broad,
        query_narrow,
        cosines,
        sines,
        (key_up_broad, value_up_broad, key_up_narrow, value_up_narrow),
    )
    both = lax.all_gather(
        jnp.concatenate([up_weight, down_weight], axis=1), "sp", axis=0, tiled=True
    )
    up_full, down_full = both[:, : up_weight.shape[1]], both[:, up_weight.shape[1] :]

    pieces = attn.reshape(2, parts, share, DB + DN).transpose(1, 0, 2, 3)
    pieces = lax.all_to_all(pieces, "tp", 0, 0, tiled=True)
    pieces = pieces.reshape(2 * parts, share, DB + DN).transpose(1, 0, 2)
    rows_broad = pieces[:, :, :DB].reshape(share, -1)
    rows_narrow = pieces[:, :, DB:].reshape(share, -1)
    projected = dot(rows_broad, out_broad) + dot(rows_narrow, out_narrow)
    own_resid = lax.dynamic_slice_in_dim(resid, lax.axis_index("tp") * share, share, 0)
    mixed = (own_resid.astype(f32) + rms_scale(projected, post_gain)).astype(bf16)
    normed = rms_scale(mixed.astype(f32), ffn_gain).astype(bf16)
    hidden = jnp.square(
        jax.nn.relu(dot(lax.all_gather(normed, "tp", axis=0, tiled=True), up_full))
    ).astype(bf16)
    ffn = dot(hidden, down_full, LAST).astype(bf16)
    ffn = lax.all_to_all(ffn.reshape(parts, share, -1), "tp", 0, 0, tiled=True)
    ffn = jnp.sum(ffn.astype(f32), axis=0)
    return (mixed.astype(f32) + rms_scale(ffn, ffn_out_gain)).astype(bf16)


def solution(mesh):
    in_specs = (
        P("sp", None),
        P("sp", "tp"),
        P("sp", "tp"),
        P("sp", None),
        P("sp", None),
        P(),
        P(None, "tp"),
        P(None, "tp"),
        P(None, "tp"),
        P(None, "tp"),
        P(),
        P(),
        P(),
        P(),
        P("sp", "tp"),
        P("sp", "tp"),
        P(),
    )
    out_specs = P(("sp", "tp"), None)
    return jax.shard_map(local, mesh=mesh, in_specs=in_specs, out_specs=out_specs, check_vma=False)
```

time: 373 us -> 215 us (0.58)
  Pallas kernels: 0 us -> 135 us
  matrix products: 142 us -> 14.2 us
  waiting for transfers between devices: 99.4 us -> 6.35 us
  other arithmetic: 55.9 us -> 8.55 us
  local copies, waits for them, and re-layouts: 21.2 us -> 2.69 us
    pallas_call x0 -> x1, Pallas kernels: none -> 135 us  [attention(): pl.pallas_call(functools.partial(attention_kernel, geometry), out_shape=j...]
    dot_general x123 -> x3, matrix products: 142 us -> 14.2 us  [dot(): return lax.dot_general(a, b, (dims, ((), ())), preferred_element_type=f32)]
    all_gather x2 -> x1, waiting for transfers between devices: 92 us -> 0.01 us  [local(): lax.all_gather(jnp.concatenate([up_weight, down_weight], axis=1), 'sp', a...]
    reduce_sum x14 -> x3, other arithmetic: 19.5 us -> 2.37 us  [rms_scale(): jnp.mean(values * values, axis=-1, keepdims=True) + norm_eps]
    split x2 -> x0, local copies, waits for them, and re-layouts: 13.7 us -> none  [sent_together(): jnp.split(lax.all_gather(both, axis, axis=dim, tiled=True), ends, axis=al...]
    reduce_sum x13 -> x1, other arithmetic: 10.7 us -> 0.12 us  [local(): ffn = jnp.sum(ffn.astype(f32), axis=0)]
    convert_element_type x19 -> x7, other arithmetic: 12.3 us -> 2.45 us  [the longest x1 1.04 us: local(): latent_normed = rms_scale(latent.astype(f32), latent_gain).astype(bf16)]
    another operation x13 -> x0, other arithmetic: 6.73 us -> none
  transfers between devices with their start and end apart: 4 -> 2, of which waited for: 3 -> 1; matrix products, arithmetic and copies ran while one was open for 55% -> 6% of each run, Pallas kernels for 0% -> 64%
where the time goes in v1:
time: 215 us; the launch traced here: 212 us
  Pallas kernels  135 us (63%)
  blocking collectives  27 us (13%)
  matrix products  14.2 us (7%)
  between operations  13.6 us (6%)
  other arithmetic  8.55 us (4%)
  waiting for transfers between devices  6.35 us (3%)
  starting transfers between devices  4.55 us (2%)
  local copies, waits for them, and re-layouts  2.69 us (1%)
    pallas_call x1, Pallas kernels, attention(): pl.pallas_call(functools.partial(attention_kernel, geometry), out_shape=j...  135 us
    all_gather x1, blocking collectives, local(): lax.all_gather(normed, 'tp', axis=0, tiled=True)  15 us
    dot_general x3, matrix products, dot(): return lax.dot_general(a, b, (dims, ((), ())), preferred_element_type=f32)  14.2 us
    all_to_all x1, blocking collectives, local(): ffn = lax.all_to_all(ffn.reshape(parts, share, -1), 'tp', 0, 0, tiled=True)  12 us
    all_to_all x1, waiting for transfers between devices, local(): pieces = lax.all_to_all(pieces, 'tp', 0, 0, tiled=True)  6.33 us
    all_to_all x1, starting transfers between devices, local(): pieces = lax.all_to_all(pieces, 'tp', 0, 0, tiled=True)  4.55 us
  transfers between devices with their start and end apart: 2, of which 1 were waited for; matrix products, arithmetic and copies ran while one was open for 6% of the time, Pallas kernels for 64%

profile of v1, /device:TPU:232, one launch (start us, length us, event | category | flops | bytes accessed | tf_op | source)
XLA Modules:
  0.0 211.6 jit_solution(12331431738752135829)
XLA Ops:
  6.5 0.0 copy-start
  6.5 0.0 all-gather.2.cloned.1.call-start
  6.5 1.8 pad_maximum_fusion
  8.4 0.0 all-gather.2.cloned.1.call-update
  8.4 0.9 copy.23
  9.4 0.3 fusion.37
  9.6 0.7 pad_maximum_fusion.2
  10.3 1.0 fusion.19
  11.4 0.5 fusion.31
  11.8 1.0 fusion.21
  12.9 0.8 pad_maximum_fusion.1.rows_hbm
  13.7 134.8 %attention.1 = bf16[2,192,192]{2,1,0:T(8,128)(2,1)} custom-call(bf16[192,640]{1,0:T(8,128)(2,1)} %pad_maximum_fusion.1.rows_hbm, bf16[192,384]{1,0:T(8,128)(2,1)} %q_broad.1, bf16[192,256]{1,0:T(8,128)(2,1)} %q_narrow.1, f32[64,384]{1,0:T(8,128)} %get-tuple-element.14.cosines, f32[64,384]{1,0:T(8,128)} %get-tuple-element.15.sines, ...), custom_call_target="tpu_custom_call" | custom-call | flops 40000000000 | bytes 20000000 | tf_op jit(solution)/shard_map/attention/pallas_call | solution.py:370
  148.5 1.6 copy.34
  150.1 0.0 copy-start.1
  150.1 4.5 %all-to-all-start = ((bf16[4,2,48,192]{3,2,1,0:T(8,128)(2,1)}), bf16[4,2,48,192]{3,2,1,0:T(8,128)(2,1)S(1)}, u32[]{:S(2)}, u32[]{:S(2)}) async-start(bf16[4,2,48,192]{3,2,1,0:T(8,128)(2,1)} %bitcast.18), calls=%async_computation | async-start | bytes 393216 | tf_op jit(solution)/shard_map/all_to_all | solution.py:476
  154.6 6.3 %all-to-all-done = bf16[4,2,48,192]{3,2,1,0:T(8,128)(2,1)S(1)} async-done(((bf16[4,2,48,192]{3,2,1,0:T(8,128)(2,1)}), bf16[4,2,48,192]{3,2,1,0:T(8,128)(2,1)S(1)}, u32[]{:S(2)}, u32[]{:S(2)}) %all-to-all-start) | async-done | bytes 147488 | tf_op jit(solution)/shard_map/all_to_all | solution.py:476
  161.0 0.1 reshape.74
  161.1 0.0 copy-start.3
  161.1 3.0 %fusion.34 = f32[48,2048]{1,0:T(8,128)S(1)} fusion(bf16[1024,2048]{1,0:T(8,128)(2,1)} %param.27, bf16[48,8,192]{2,0,1:T(8,128)(2,1)S(1)} %bitcast.21), kind=kOutput, calls=%fused_computation.39 | convolution fusion | flops 201326592 | bytes 4685824 | tf_op jit(solution)/shard_map/dot_general | solution.py:25
  164.2 0.0 copy-done
  164.2 0.6 multiply_reduce_fusion.1
  164.8 0.0 copy-done.1
  164.8 1.2 fusion.22
  166.0 0.0 copy-done.3
  166.0 0.1 fusion.24
  166.1 15.0 %all_gather.6 = bf16[192,2048]{1,0:T(8,128)(2,1)} all-gather(bf16[48,2048]{1,0:T(8,128)(2,1)S(1)} %fusion.24), channel_id=1, replica_groups=mesh['sp'=64,'tp'=4] {'tp'}, dimensions={0}, use_global_device_ids=true | all-gather | bytes 983040 | tf_op jit(solution)/shard_map/all_gather | solution.py:485
  181.1 10.6 %fusion.10 = bf16[192,2048]{1,0:T(8,128)(2,1)S(1)} fusion(bf16[2048,4096]{1,0:T(8,128)(2,1)} %all-gather.2.cloned.1.call-done, bf16[192,2048]{1,0:T(8,128)(2,1)} %all_gather.6), kind=kOutput, calls=%fused_computation.6 | convolution fusion | flops 3222798336 | bytes 18350080 | tf_op jit(solution)/shard_map/dot_general | solution.py:25
  191.7 12.0 %all_to_all.10 = bf16[4,48,2048]{2,1,0:T(8,128)(2,1)S(1)} all-to-all(bf16[4,48,2048]{2,1,0:T(8,128)(2,1)S(1)} %bitcast.19), channel_id=1, replica_groups=mesh['sp'=64,'tp'=4] {'tp'}, dimensions={0} | all-to-all | bytes 1572864 | tf_op jit(solution)/shard_map/all_to_all | solution.py:488
  203.7 0.1 convert_reduce_fusion
  203.8 0.1 multiply_reduce_fusion
  204.0 0.0 copy-done.2
  204.0 0.8 fusion.25
  (14 shorter events, 0.1 us)
Async XLA Ops:
  6.5 157.7 %copy-start = (bf16[512,2048]{1,0:T(8,128)(2,1)S(1)}, bf16[512,2048]{1,0:T(8,128)(2,1)}, u32[]{:S(2)}) copy-start(bf16[512,2048]{1,0:T(8,128)(2,1)} %param.28) | copy-start | bytes 6291460
  6.5 174.6 %all-gather.2.cloned.1.call-start = ((), (), s32[]{:S(2)}) async-start(), calls=%async_computation.2 | async-start | bytes 17039360 | tf_op jit(solution)/shard_map/all_gather | solution.py:470
  150.1 14.7 %copy-start.1 = (f32[2048]{0:T(1024)S(1)}, f32[2048]{0:T(1024)}, u32[]{:S(2)}) copy-start(f32[2048]{0:T(1024)} %param.29) | copy-start | bytes 24580
  150.1 10.9 %all-to-all-start = ((bf16[4,2,48,192]{3,2,1,0:T(8,128)(2,1)}), bf16[4,2,48,192]{3,2,1,0:T(8,128)(2,1)S(1)}, u32[]{:S(2)}, u32[]{:S(2)}) async-start(bf16[4,2,48,192]{3,2,1,0:T(8,128)(2,1)} %bitcast.18), calls=%async_computation | async-start | bytes 393216 | tf_op jit(solution)/shard_map/all_to_all | solution.py:476
  161.1 4.9 %copy-start.3 = (f32[2048]{0:T(1024)S(1)}, f32[2048]{0:T(1024)}, u32[]{:S(2)}) copy-start(f32[2048]{0:T(1024)} %param.30) | copy-start | bytes 24580
  181.1 22.9 %copy-start.2 = (f32[2048]{0:T(1024)S(1)}, f32[2048]{0:T(1024)}, u32[]{:S(2)}) copy-start(f32[2048]{0:T(1024)} %param.33) | copy-start | bytes 24580
Sparse Core Ops, SparseCore 0:
  10.1 121.8 all-gather.1

commit v2 on v1

--- a/solution.py
+++ b/solution.py
@@ -201,18 +201,27 @@
     def begin(self):
         self.start(*self.both("ay", 0), *self.both("bz", 0))
 
-    def open_rings(self):
+    def open_y(self):
         self.landed(*self.both("ay", 0))
         self.start(*self.both("ay", 1))
-        self.landed(*self.both("bz", 0))
-        self.start(*self.both("bz", 1))
+
+    def open_z(self):
         self.landed(*self.both("ay", 1))
         self.start(*self.both("az", 0), *self.both("pa", -1))
+
+    def next_z(self, s):
+        self.landed(*self.both("bz", s))
+        if s + 1 < self.half_z:
+            self.start(*self.both("bz", s + 1))
+        else:
+            self.start(*self.both("by", 0), *self.both("pb", -1))
+
+    def open_rings(self):
+        self.open_y()
+        self.next_z(0)
+        self.open_z()
         for s in range(1, self.half_z):
-            self.landed(*self.both("bz", s))
-            if s + 1 < self.half_z:
-                self.start(*self.both("bz", s + 1))
-        self.start(*self.both("by", 0), *self.both("pb", -1))
+            self.next_z(s)
 
     def pass_on(self, name):
         kind, s, d, ch = name
@@ -243,7 +252,11 @@
             self.copy(name).wait_send()
 
 
-def attention_kernel(
+MESH = pl.DeviceIdType.MESH
+CHUNK = 512
+
+
+def layer_kernel(
     geometry,
     rows_hbm,
     q_broad,
@@ -254,8 +267,17 @@
     value_up_broad,
     key_up_narrow,
     value_up_narrow,
+    post_gain,
+    ffn_gain,
+    ffn_out_gain,
+    resid_hbm,
+    out_broad_hbm,
+    out_narrow_hbm,
+    up_hbm,
+    down_hbm,
     out,
     held,
+    weights,
     all_q_broad,
     all_q_narrow,
     qt_broad,
@@ -266,52 +288,101 @@
     total,
     acc,
     finished,
-    own_sem,
+    gathered,
+    out_broad,
+    out_narrow,
+    resid,
+    wide,
+    mixed,
+    normed,
+    hidden,
+    partial,
+    partial_sent,
+    relayed,
+    combined,
+    from_far,
+    from_near,
+    local_sem,
     sent,
     arrived,
-    more_sent,
-    more_arrived,
+    w_sent,
+    w_arrived,
+    q_sent,
+    q_arrived,
+    a_sent,
+    a_arrived,
+    n_sent,
+    n_arrived,
+    r_sent,
+    r_arrived,
 ):
-    nz, ny, first, first_cut, rest_cut = geometry
-    me = lax.axis_index("sp")
+    nz, ny, parts, cuts, w_cuts = geometry
+    me, x = lax.axis_index("sp"), lax.axis_index("tp")
     core = lax.rem(me, 2)
     chip = me // 2
     z, y = chip // ny, lax.rem(chip, ny)
     rows = rows_hbm.shape[0]
-    zs, ys = ring_places(nz), ring_places(ny)
-    spread = Spread(held, sent, arrived, (z, y, core), first, first_cut, rest_cut)
-
-    own = pltpu.make_async_copy(rows_hbm, held.at[z, y, core], own_sem)
-    own.start()
+    share = rows // parts
+    zs, ys, xs = ring_places(nz), ring_places(ny), ring_places(parts)
+    spread = Spread(held, sent, arrived, (z, y, core), *cuts)
+    w_spread = Spread(weights, w_sent, w_arrived, (z, y, core), *w_cuts)
+    model_rows = up_hbm.shape[0]
+
+    own_rows = pltpu.make_async_copy(rows_hbm, held.at[z, y, core], local_sem.at[0])
+    own_rows.start()
+    loads = [
+        (up_hbm, weights.at[z, y, core, pl.ds(0, model_rows)]),
+        (down_hbm, weights.at[z, y, core, pl.ds(model_rows, model_rows)]),
+        (out_broad_hbm, out_broad),
+        (out_narrow_hbm, out_narrow),
+        (resid_hbm.at[pl.ds(x * share, share)], resid),
+    ]
+    loads = [
+        pltpu.make_async_copy(src, dst, local_sem.at[i + 1]) for i, (src, dst) in enumerate(loads)
+    ]
+    for load in loads:
+        load.start()
+
+    def tile_peer(offset):
+        there = lax.rem(core * parts + x + offset, 2 * parts)
+        return there, {
+            "sp": (z * ny + y) * 2 + there // parts,
+            "tp": lax.rem(there, parts),
+        }
+
     barrier = pltpu.get_barrier_semaphore()
-    neighbours = [
-        spread.device(z, y, 1 - core),
+    neighbours = [tile_peer(offset)[1] for offset in range(1, 2 * parts)] + [
         spread.device(z, ys(y, 1), core),
         spread.device(z, ys(y, -1), core),
         spread.device(zs(z, 1), y, core),
         spread.device(zs(z, -1), y, core),
     ]
     for neighbour in neighbours:
-        pl.semaphore_signal(
-            barrier, inc=1, device_id=neighbour, device_id_type=pl.DeviceIdType.MESH
-        )
+        pl.semaphore_signal(barrier, inc=1, device_id=neighbour, device_id_type=MESH)
     pl.semaphore_wait(barrier, len(neighbours))
-    own.wait()
+    own_rows.wait()
     spread.begin()
 
-    def to_partner(src, dst, i):
+    def remote(src, dst, sems, i, device):
         return pltpu.make_async_remote_copy(
             src_ref=src,
             dst_ref=dst,
-            send_sem=more_sent.at[i],
-            recv_sem=more_arrived.at[i],
-            device_id=spread.device(z, y, 1 - core),
-            device_id_type=pl.DeviceIdType.MESH,
+            send_sem=sems[0].at[i],
+            recv_sem=sems[1].at[i],
+            device_id=device,
+            device_id_type=MESH,
         )
 
+    partner = spread.device(z, y, 1 - core)
+    q_sems, a_sems, n_sems, r_sems = (
+        (q_sent, q_arrived),
+        (a_sent, a_arrived),
+        (n_sent, n_arrived),
+        (r_sent, r_arrived),
+    )
     exchange = [
-        to_partner(q_broad, all_q_broad.at[core], 0),
-        to_partner(q_narrow, all_q_narrow.at[core], 1),
+        remote(q_broad, all_q_broad.at[core], q_sems, 0, partner),
+        remote(q_narrow, all_q_narrow.at[core], q_sems, 1, partner),
     ]
     for copy in exchange:
         copy.start()
@@ -339,43 +410,197 @@
         return held[k // ny, lax.rem(k, ny)].reshape(2 * rows, -1)
 
     attend_block(block_of(chip), True, *tools)
+    for load in loads:
+        load.wait()
     for name in spread.order():
         spread.pass_on(name)
+    w_spread.begin()
     spread.landed(*spread.handed())
 
+    def opening():
+        w_spread.open_y()
+        w_spread.next_z(0)
+
+    def opened():
+        w_spread.open_z()
+        w_spread.next_z(1)
+
+    turns = {3: opening, 7: opened}
+    at = 10
+    for s in range(2, w_spread.half_z):
+        turns[at] = functools.partial(w_spread.next_z, s)
+        at += 3
+    w_order = w_spread.order()
+    early, late = w_order[:4], w_order[4:]
+    for i, name in enumerate(early):
+        turns[20 + i] = functools.partial(w_spread.pass_on, name)
+
     def earlier(k, carried):
-        attend_block(block_of(k), False, *tools)
+        for turn, action in turns.items():
+            pl.when(k == turn)(action)
+
+        @pl.when(k < chip)
+        def _():
+            attend_block(block_of(k), False, *tools)
+
         return carried
 
-    lax.fori_loop(0, chip, earlier, 0)
+    lax.fori_loop(0, nz * ny, earlier, 0)
+
+    def more_turns(count):
+        for _ in range(min(count, len(late))):
+            w_spread.pass_on(late.pop(0))
+
     broad = jnp.transpose(acc[0:DB] / total[0])
     narrow = jnp.transpose(acc[DB : DB + DN] / total[1])
     finished[...] = (
-        jnp.concatenate([broad, narrow], axis=1).astype(bf16).reshape(2, rows, DB + DN)
+        jnp.concatenate([broad, narrow], axis=1).astype(bf16).reshape(2 * parts, share, DB + DN)
     )
-    result = to_partner(finished.at[1 - core], out.at[core], 2)
-    result.start()
-    out[core] = finished[core]
+    mine = core * parts + x
+    pair = 2 * x + core
+    to_owners = []
+    for offset in range(1, 2 * parts):
+        there, device = tile_peer(offset)
+        to_owners.append(remote(finished.at[there], gathered.at[pair], a_sems, offset - 1, device))
+    for copy in to_owners:
+        copy.start()
+    gathered[pair] = finished[mine]
+    more_turns(4)
+    for copy in to_owners:
+        copy.wait_recv()
+    rows_broad = jnp.concatenate([gathered[g, :, 0:DB] for g in range(2 * parts)], axis=1)
+    rows_narrow = jnp.concatenate([gathered[g, :, DB : DB + DN] for g in range(2 * parts)], axis=1)
+    width = out.shape[1]
+
+    def project(n, carried):
+        columns = pl.ds(pl.multiple_of(n * CHUNK, CHUNK), CHUNK)
+        wide[:, columns] = dot(rows_broad, out_broad[:, columns]) + dot(
+            rows_narrow, out_narrow[:, columns]
+        )
+        return carried
+
+    lax.fori_loop(0, width // CHUNK, project, 0)
+    mix = (resid[...].astype(f32) + rms_scale(wide[...], post_gain[...])).astype(bf16)
+    mixed[...] = mix
+    normed[x] = rms_scale(mix.astype(f32), ffn_gain[...]).astype(bf16)
+    right, left = {"tp": xs(x, 1)}, {"tp": xs(x, -1)}
+    first_rows, last_rows = pl.ds(0, 32), pl.ds(32, share - 32)
+    around = [
+        remote(normed.at[x], normed.at[x], n_sems, 0, right),
+        remote(normed.at[x], normed.at[x], n_sems, 1, left),
+        remote(
+            normed.at[xs(x, -1), first_rows], normed.at[xs(x, -1), first_rows], n_sems, 2, right
+        ),
+        remote(normed.at[xs(x, 1), last_rows], normed.at[xs(x, 1), last_rows], n_sems, 3, left),
+    ]
+    around[0].start()
+    around[1].start()
+    more_turns(4)
+    around[0].wait_recv()
+    around[2].start()
+    around[1].wait_recv()
+    around[3].start()
+    more_turns(len(late))
+    around[2].wait_recv()
+    around[3].wait_recv()
+    w_spread.landed(*w_spread.own_chip(), *w_spread.handed())
+    inputs = normed[...].reshape(rows, width)
+
+    def raise_up(n, carried):
+        columns = pl.ds(pl.multiple_of(n * CHUNK, CHUNK), CHUNK)
+        up = weights[:, :, :, 0:model_rows, columns].reshape(width, CHUNK)
+        raised = jnp.maximum(dot(inputs, up), 0.0)
+        hidden[:, columns] = (raised * raised).astype(bf16)
+        return carried
+
+    lax.fori_loop(0, hidden.shape[1] // CHUNK, raise_up, 0)
+
+    pieces = width // CHUNK
+    per_z = 2 * ny * model_rows
+    copies = {}
+    for n in range(pieces):
+        d = 1 if n % 2 == 0 else -1
+        columns = slice(n * CHUNK, (n + 1) * CHUNK)
+        near, far = {"tp": xs(x, d)}, {"tp": xs(x, -d)}
+        copies[n] = (
+            remote(partial_sent.at[xs(x, 2), :, columns], relayed.at[n], r_sems, 3 * n, near),
+            remote(
+                partial_sent.at[xs(x, -d), :, columns],
+                from_near.at[:, columns],
+                r_sems,
+                3 * n + 1,
+                far,
+            ),
+            remote(combined.at[n], from_far.at[:, columns], r_sems, 3 * n + 2, near),
+        )
+
+    def lower(n):
+        columns = slice(n * CHUNK, (n + 1) * CHUNK)
+        zn = CHUNK // per_z
+        down = weights[n * zn : (n + 1) * zn, :, :, model_rows : 2 * model_rows].reshape(
+            CHUNK, hidden.shape[1]
+        )
+        sums = dot(hidden[...], down, LAST).reshape(parts, share, CHUNK)
+        partial[:, :, columns] = sums
+        partial_sent[:, :, columns] = sums.astype(bf16)
+        copies[n][0].start()
+        copies[n][1].start()
+
+    def relay(n):
+        d = 1 if n % 2 == 0 else -1
+        columns = slice(n * CHUNK, (n + 1) * CHUNK)
+        copies[n][0].wait_recv()
+        combined[n] = (partial[xs(x, d), :, columns] + relayed[n].astype(f32)).astype(bf16)
+        copies[n][2].start()
+
+    for n in range(pieces):
+        lower(n)
+        if n > 0:
+            relay(n - 1)
+    relay(pieces - 1)
+    for n in range(pieces):
+        copies[n][1].wait_recv()
+        copies[n][2].wait_recv()
+    ffn = partial[x] + from_near[...].astype(f32) + from_far[...].astype(f32)
+    out[...] = (mixed[...].astype(f32) + rms_scale(ffn, ffn_out_gain[...])).astype(bf16)
     spread.drain()
-    for copy in exchange:
+    w_spread.drain()
+    for copy in exchange + to_owners + around:
         copy.wait_send()
-    result.wait()
-
-
-def attention(geometry, packed, q_broad, q_narrow, cosines, sines, ups):
-    nz, ny = geometry[:2]
-    rows, width = packed.shape
+    for n in range(pieces):
+        for copy in copies[n]:
+            copy.wait_send()
+
+
+def rms_scale(values, norm_gain):
+    return (
+        values * lax.rsqrt(jnp.mean(values * values, axis=-1, keepdims=True) + norm_eps) * norm_gain
+    )
+
+
+def layer(geometry, packed, queries, tables, ups, gains, resid, outs, up_weight, down_weight):
+    nz, ny, parts = geometry[:3]
+    rows, latent_width = packed.shape
+    width = resid.shape[1]
+    hidden = up_weight.shape[1]
+    share = rows // parts
+    model_rows = up_weight.shape[0]
     vmem = pl.BlockSpec(memory_space=pltpu.VMEM)
+    anywhere = pl.BlockSpec(memory_space=pl.ANY)
     copies = Spread.count(nz, ny)
+    pieces = width // CHUNK
+    sems = pltpu.SemaphoreType.DMA
+    operands = (packed, *queries, *tables, *ups, *gains, resid, *outs, up_weight, down_weight)
     return pl.pallas_call(
-        functools.partial(attention_kernel, geometry),
-        out_shape=jax.ShapeDtypeStruct((2, rows, DB + DN), bf16),
-        in_specs=[pl.BlockSpec(memory_space=pl.ANY)] + [vmem] * 8,
+        functools.partial(layer_kernel, geometry),
+        out_shape=jax.ShapeDtypeStruct((share, width), bf16),
+        in_specs=[anywhere] + [vmem] * 11 + [anywhere] * 5,
         out_specs=vmem,
         scratch_shapes=[
-            pltpu.VMEM((nz, ny, 2, rows, width), bf16),
-            pltpu.VMEM((2, rows, q_broad.shape[1]), bf16),
-            pltpu.VMEM((2, rows, q_narrow.shape[1]), bf16),
+            pltpu.VMEM((nz, ny, 2, rows, latent_width), bf16),
+            pltpu.VMEM((nz, ny, 2, 2 * model_rows, hidden), bf16),
+            pltpu.VMEM((2, rows, queries[0].shape[1]), bf16),
+            pltpu.VMEM((2, rows, queries[1].shape[1]), bf16),
             pltpu.VMEM((256, 2 * rows), bf16),
             pltpu.VMEM((128, 2 * rows), bf16),
             pltpu.VMEM((512, 256), bf16),
@@ -383,27 +608,43 @@
             pltpu.VMEM((2, 1, 2 * rows), f32),
             pltpu.VMEM((2, 1, 2 * rows), f32),
             pltpu.VMEM((DB + DN, 2 * rows), f32),
-            pltpu.VMEM((2, rows, DB + DN), bf16),
-            pltpu.SemaphoreType.DMA,
-            pltpu.SemaphoreType.DMA((copies,)),
-            pltpu.SemaphoreType.DMA((copies,)),
-            pltpu.SemaphoreType.DMA((3,)),
-            pltpu.SemaphoreType.DMA((3,)),
+            pltpu.VMEM((2 * parts, share, DB + DN), bf16),
+            pltpu.VMEM((2 * parts, share, DB + DN), bf16),
+            pltpu.VMEM(outs[0].shape, bf16),
+            pltpu.VMEM(outs[1].shape, bf16),
+            pltpu.VMEM((share, width), bf16),
+            pltpu.VMEM((share, width), f32),
+            pltpu.VMEM((share, width), bf16),
+            pltpu.VMEM((parts, share, width), bf16),
+            pltpu.VMEM((rows, hidden), bf16),
+            pltpu.VMEM((parts, share, width), f32),
+            pltpu.VMEM((parts, share, width), bf16),
+            pltpu.VMEM((pieces, share, CHUNK), bf16),
+            pltpu.VMEM((pieces, share, CHUNK), bf16),
+            pltpu.VMEM((share, width), bf16),
+            pltpu.VMEM((share, width), bf16),
+            sems((6,)),
+            sems((copies,)),
+            sems((copies,)),
+            sems((copies,)),
+            sems((copies,)),
+            sems((2,)),
+            sems((2,)),
+            sems((2 * parts - 1,)),
+            sems((2 * parts - 1,)),
+            sems((4,)),
+            sems((4,)),
+            sems((3 * pieces,)),
+            sems((3 * pieces,)),
         ],
         compiler_params=pltpu.CompilerParams(
-            collective_id=0, has_side_effects=True, vmem_limit_bytes=56 * 1024 * 1024
+            collective_id=0, has_side_effects=True, vmem_limit_bytes=63 * 1024 * 1024
         ),
         cost_estimate=pl.CostEstimate(
             flops=40_000_000_000, bytes_accessed=20_000_000, transcendentals=9_000_000
         ),
-        name="attention",
-    )(packed, q_broad, q_narrow, cosines, sines, *ups)
-
-
-def rms_scale(values, norm_gain):
-    return (
-        values * lax.rsqrt(jnp.mean(values * values, axis=-1, keepdims=True) + norm_eps) * norm_gain
-    )
+        name="layer",
+    )(*operands)
 
 
 def angles_of(first, count):
@@ -433,10 +674,8 @@
 ):
     rows = resid.shape[0]
     parts = lax.axis_size("tp")
-    share = rows // parts
     me = lax.axis_index("sp")
-    ny = NY
-    nz = lax.axis_size("sp") // (2 * ny)
+    nz = lax.axis_size("sp") // (2 * NY)
 
     positions, frequency = angles_of(me * rows, rows)
     angles = positions[:, None] * frequency[None, :]
@@ -457,37 +696,18 @@
     cosine, sine = jnp.cos(angles), jnp.sin(angles)
     cosines = jnp.concatenate([cosine, cosine], axis=0)
     sines = jnp.concatenate([-sine, sine], axis=0)
-    geometry = (nz, ny, 80, 48, 64)
-    attn = attention(
-        geometry,
+    return layer(
+        (nz, NY, parts, (80, 48, 64), (32, 16, 16)),
         packed,
-        query_broad,
-        query_narrow,
-        cosines,
-        sines,
+        (query_broad, query_narrow),
+        (cosines, sines),
         (key_up_broad, value_up_broad, key_up_narrow, value_up_narrow),
+        (post_gain[None, :], ffn_gain[None, :], ffn_out_gain[None, :]),
+        resid,
+        (out_broad, out_narrow),
+        up_weight,
+        down_weight,
     )
-    both = lax.all_gather(
-        jnp.concatenate([up_weight, down_weight], axis=1), "sp", axis=0, tiled=True
-    )
-    up_full, down_full = both[:, : up_weight.shape[1]], both[:, up_weight.shape[1] :]
-
-    pieces = attn.reshape(2, parts, share, DB + DN).transpose(1, 0, 2, 3)
-    pieces = lax.all_to_all(pieces, "tp", 0, 0, tiled=True)
-    pieces = pieces.reshape(2 * parts, share, DB + DN).transpose(1, 0, 2)
-    rows_broad = pieces[:, :, :DB].reshape(share, -1)
-    rows_narrow = pieces[:, :, DB:].reshape(share, -1)
-    projected = dot(rows_broad, out_broad) + dot(rows_narrow, out_narrow)
-    own_resid = lax.dynamic_slice_in_dim(resid, lax.axis_index("tp") * share, share, 0)
-    mixed = (own_resid.astype(f32) + rms_scale(projected, post_gain)).astype(bf16)
-    normed = rms_scale(mixed.astype(f32), ffn_gain).astype(bf16)
-    hidden = jnp.square(
-        jax.nn.relu(dot(lax.all_gather(normed, "tp", axis=0, tiled=True), up_full))
-    ).astype(bf16)
-    ffn = dot(hidden, down_full, LAST).astype(bf16)
-    ffn = lax.all_to_all(ffn.reshape(parts, share, -1), "tp", 0, 0, tiled=True)
-    ffn = jnp.sum(ffn.astype(f32), axis=0)
-    return (mixed.astype(f32) + rms_scale(ffn, ffn_out_gain)).astype(bf16)
 
 
 def solution(mesh):

time: 215 us -> 172 us (0.80)
  the two profiles are of different devices: /device:TPU:232 before, /device:TPU:28 now
where the time goes in v2:
time: 172 us
  Pallas kernels  165 us (96%)
  other arithmetic  4.31 us (3%)
  local copies, waits for them, and re-layouts  2.49 us (1%)
    pallas_call x1, Pallas kernels, layer(): pl.pallas_call(functools.partial(layer_kernel, geometry), out_shape=jax.S...  165 us

profile of v2, /device:TPU:28, one launch (start us, length us, event | category | flops | bytes accessed | tf_op | source)
XLA Modules:
  0.0 171.7 jit_solution(3785461628127100550)
XLA Ops:
  0.0 0.9 copy.19
  0.9 0.5 fusion.8
  1.4 1.0 fusion
  2.4 1.0 fusion.2
  3.5 0.8 pad_maximum_fusion.rows_hbm
  4.3 0.3 fusion.11
  4.6 0.7 pad_maximum_fusion.1
  5.3 164.8 %layer.1 = bf16[48,2048]{1,0:T(8,128)(2,1)} custom-call(bf16[192,640]{1,0:T(8,128)(2,1)} %pad_maximum_fusion.rows_hbm, bf16[192,384]{1,0:T(8,128)(2,1)} %q_broad.1, bf16[192,256]{1,0:T(8,128)(2,1)} %q_narrow.1, f32[64,384]{1,0:T(8,128)} %get-tuple-element.10.cosines, f32[64,384]{1,0:T(8,128)} %get-tuple-element.11.sines, bf16[512,256]{1,0:T(8,128)(2,1)} %key_up_broad.1, ...), custom_call_target="tpu_custom_call" | custom-call | flops 40000000000 | bytes 20000000 | tf_op jit(solution)/shard_map/layer/pallas_call | solution.py:594
  170.1 1.6 copy.22
  (7 shorter events, 0.1 us)

commit v3 on v2

--- a/solution.py
+++ b/solution.py
@@ -113,71 +113,160 @@
     return lambda at, step: lax.rem(at + step + axis_size, axis_size)
 
 
-class Spread:
-    def __init__(self, held, sent, arrived, place, first, first_cut, rest_cut):
-        self.held, self.sent, self.arrived = held, sent, arrived
-        self.z, self.y, self.core = place
-        self.nz, self.ny, _, self.rows, _ = held.shape
-        self.first, self.first_cut, self.rest_cut = first, first_cut, rest_cut
-        self.half_z, self.half_y = self.nz // 2, self.ny // 2
-        names = [("ay", s, d) for s in (0, 1) for d in (1, -1)]
-        for s in range(self.half_z):
+def offset_of(k):
+    return (k + 1) // 2 * (1 if k % 2 else -1)
+
+
+Y_BLOCKS = (0, -1, 1, 2)
+
+
+def copies_of(nz, ny, crossed):
+    assert ny == 4 and nz % 4 == 0
+    last = nz // 2 - 1
+    tasks = {}
+    for d in (1, -1):
+        tasks["ay", 0, d] = (("y", d), "a", 1, ())
+        tasks["ay", 1, d] = (("y", d), "a" + "+-"[d < 0], 1, (("ay", 0, d),))
+    source = {0: (), -1: (("ay", 0, 1),), 1: (("ay", 0, -1),), 2: (("ay", 1, 1), ("ay", 1, -1))}
+    for s in range(last + 1):
+        for j, at in enumerate(Y_BLOCKS):
             for d in (1, -1):
-                names.append(("bz", s, d))
-                for ch in (0, 1):
-                    if s < self.half_z - 1 or ch == (0 if d == 1 else 1):
-                        names.append(("az", s, d, ch))
-                        names.append(("pa", s, d, ch))
-        for s in (0, 1):
+                if s < last or d == (1 if j % 2 == 0 else -1):
+                    before = source[at] if s == 0 else (("az", s - 1, d, j),)
+                    tasks["az", s, d, j] = (("z", d), "a", 1, before)
+        for d in (1, -1):
+            rows = "b" if s < last else "b" + "+-"[d < 0]
+            tasks["bz", s, d] = (("z", d), rows, 1, () if s == 0 else (("bz", s - 1, d),))
+    planes = {}
+    for k in range(nz):
+        off = offset_of(k)
+        came = -1 if off > 0 else 1
+        if k == 0:
+            column, plane = (), tuple(tasks_ for tasks_ in tasks if tasks_[0] == "ay")
+        elif k == nz - 1:
+            column = (("bz", last, 1), ("bz", last, -1))
+            plane = tuple(("az", last, 1 if j % 2 == 0 else -1, j) for j in range(ny)) + column
+        else:
+            column = (("bz", abs(off) - 1, came),)
+            plane = tuple(("az", abs(off) - 1, came, j) for j in range(ny)) + column
+        far = 1 if k % 2 == 0 else -1
+        for d in (1, -1):
+            tasks["by", k, 0, d] = (("y", d), "b", 1, column)
+        tasks["by", k, 1, far] = (("y", far), "b", 1, (("by", k, 0, far),))
+        plane += (("by", k, 0, 1), ("by", k, 0, -1), ("by", k, 1, far))
+        tasks["hand", k] = (("c", 0), "ab", ny, plane)
+        if crossed:
             for d in (1, -1):
-                for ch in (0, 1):
-                    if s == 0 or ch == (0 if d == 1 else 1):
-                        names.append(("by", s, d, ch))
-                        names.append(("pb", s, d, ch))
-        names += [("pa", -1, 1, 0), ("pa", -1, 1, 1), ("pb", -1, 1, 0)]
-        self.index = {name: i for i, name in enumerate(names)}
-
-    @staticmethod
-    def count(nz, ny):
-        return 4 + (nz // 2) * 2 + 2 * ((nz // 2 - 1) * 4 + 2) + 2 * 6 + 3
+                tasks["x", k, d] = (("x", d), "ab", ny // 2, plane)
+            tasks["handx", k] = (("c", 0), "ab", ny, (("x", k, 1), ("x", k, -1)))
+            plane += (("x", k, 1), ("x", k, -1), ("handx", k))
+        planes[k] = plane + (("hand", k),)
+    return tasks, planes
+
+
+def foreseen(groups, delays, link_rate=46.0, chip_rate=450.0, latency=2.0):
+    landed, waiting, free, now = {}, set(), {}, 0.0
+    pending = []
+    for g, (tasks, sizes) in groups.items():
+        for name in tasks:
+            waiting.add((g, name))
+    started = set()
+
+    def start_ready(time):
+        for g, (tasks, sizes) in groups.items():
+            if time < delays[g]:
+                continue
+            for name, (link, rows, blocks, before) in tasks.items():
+                key = (g, name)
+                if key in started or any((g, b) not in landed for b in before):
+                    continue
+                started.add(key)
+                rate = chip_rate if link[0] == "c" else link_rate
+                begin = max(time, free.get(link, 0.0))
+                end = begin + sizes[rows] * blocks / rate / 1e3
+                free[link] = end
+                pending.append((end + (1.0 if link[0] == "c" else latency), key))
+
+    times = sorted(set(delays.values()))
+    while True:
+        for t in times:
+            if t <= now:
+                start_ready(now)
+        later = [t for t in times if t > now]
+        upcoming = min(pending)[0] if pending else None
+        if upcoming is None and not later:
+            break
+        if upcoming is None or (later and later[0] < upcoming):
+            now = later[0]
+            continue
+        pending.sort()
+        now, key = pending.pop(0)
+        landed[key] = now
+    return landed
+
+
+class Web:
+    def __init__(self, held, sems, place, tasks, cuts, crossed):
+        self.held, self.sent, self.arrived = held, *sems
+        self.z, self.y, self.core, self.x, self.parts = place
+        self.nz, self.ny = held.shape[:2]
+        self.tasks = tasks
+        self.index = {name: i for i, name in enumerate(tasks)}
+        a, b, a_cut, b_cut = cuts
+        self.spans = {
+            "a": (0, a),
+            "b": (a, b),
+            "a+": (0, a_cut),
+            "a-": (a_cut, a - a_cut),
+            "b+": (a, b_cut),
+            "b-": (a + b_cut, b - b_cut),
+            "ab": (0, a + b),
+        }
+        parity = lax.rem(self.x, 2) if crossed else 0
+        self.base = parity * (a + b)
+        self.other_base = (1 - parity) * (a + b)
+
+    def sizes(self):
+        row = self.held.shape[4] * 2
+        return {key: size * row for key, (_, size) in self.spans.items()}
+
+    def rows(self, key, base):
+        start, size = self.spans[key]
+        if isinstance(base, int):
+            return pl.ds(base + start, size)
+        return pl.ds(pl.multiple_of(base + start, 16), size)
 
     def device(self, z, y, core):
         return {"sp": (z * self.ny + y) * 2 + core}
 
     def copy(self, name):
-        kind, s, d = name[:3]
-        zs, ys = ring_places(self.nz), ring_places(self.ny)
-        z, y, c, held, first = self.z, self.y, self.core, self.held, self.first
-        low, high = pl.ds(0, first), pl.ds(first, self.rows - first)
+        kind = name[0]
+        link, key, _, _ = self.tasks[name]
+        zs, ys, xs = ring_places(self.nz), ring_places(self.ny), ring_places(self.parts)
+        z, y, c = self.z, self.y, self.core
+        rows = self.rows(key, self.other_base if kind == "handx" else self.base)
+        if kind == "ay":
+            at = (z, ys(y, -name[1] * name[2]))
+        elif kind == "az":
+            at = (zs(z, -name[1] * name[2]), ys(y, Y_BLOCKS[name[3]]))
+        elif kind == "bz":
+            at = (zs(z, -name[1] * name[2]), y)
+        elif kind == "by":
+            at = (zs(z, offset_of(name[1])), ys(y, -name[2] * name[3]))
+        elif kind == "x":
+            half = self.ny // 2
+            at = (zs(z, offset_of(name[1])), pl.ds(0 if name[2] == 1 else half, half))
+        else:
+            at = (zs(z, offset_of(name[1])), pl.ds(0, self.ny))
+        view = self.held.at[at[0], at[1], c, rows]
+        axis, d = link
+        to = {
+            "y": lambda: self.device(z, ys(y, d), c),
+            "z": lambda: self.device(zs(z, d), y, c),
+            "c": lambda: self.device(z, y, 1 - c),
+            "x": lambda: {"tp": xs(self.x, d)},
+        }[axis]()
         i = self.index[name]
-        if kind == "ay":
-            if s == 1:
-                low = (
-                    pl.ds(0, self.first_cut)
-                    if d == 1
-                    else pl.ds(self.first_cut, first - self.first_cut)
-                )
-            view, to = held.at[z, ys(y, -s * d), c, low], self.device(z, ys(y, d), c)
-        elif kind == "bz":
-            if s == self.half_z - 1:
-                high = (
-                    pl.ds(first, self.rest_cut)
-                    if d == 1
-                    else pl.ds(first + self.rest_cut, self.rows - first - self.rest_cut)
-                )
-            view, to = held.at[zs(z, -s * d), y, c, high], self.device(zs(z, d), y, c)
-        elif kind == "az":
-            part = pl.ds(name[3] * self.half_y, self.half_y)
-            view, to = held.at[zs(z, -s * d), part, c, low], self.device(zs(z, d), y, c)
-        elif kind == "by":
-            part = pl.ds(name[3] * self.half_z, self.half_z)
-            view, to = held.at[part, ys(y, -s * d), c, high], self.device(z, ys(y, d), c)
-        elif kind == "pa":
-            part = pl.ds(name[3] * self.half_y, self.half_y)
-            view, to = held.at[zs(z, -(s + 1) * d), part, c, low], self.device(z, y, 1 - c)
-        else:
-            part = pl.ds(0, self.nz) if s == -1 else pl.ds(name[3] * self.half_z, self.half_z)
-            view, to = held.at[part, ys(y, -(s + 1) * d), c, high], self.device(z, y, 1 - c)
         return pltpu.make_async_remote_copy(
             src_ref=view,
             dst_ref=view,
@@ -187,73 +276,37 @@
             device_id_type=pl.DeviceIdType.MESH,
         )
 
-    def start(self, *names):
-        for name in names:
-            self.copy(name).start()
-
-    def landed(self, *names):
-        for name in names:
-            self.copy(name).wait_recv()
-
-    def both(self, kind, s):
-        return [n for n in self.index if n[0] == kind and n[1] == s]
-
-    def begin(self):
-        self.start(*self.both("ay", 0), *self.both("bz", 0))
-
-    def open_y(self):
-        self.landed(*self.both("ay", 0))
-        self.start(*self.both("ay", 1))
-
-    def open_z(self):
-        self.landed(*self.both("ay", 1))
-        self.start(*self.both("az", 0), *self.both("pa", -1))
-
-    def next_z(self, s):
-        self.landed(*self.both("bz", s))
-        if s + 1 < self.half_z:
-            self.start(*self.both("bz", s + 1))
-        else:
-            self.start(*self.both("by", 0), *self.both("pb", -1))
-
-    def open_rings(self):
-        self.open_y()
-        self.next_z(0)
-        self.open_z()
-        for s in range(1, self.half_z):
-            self.next_z(s)
-
-    def pass_on(self, name):
-        kind, s, d, ch = name
-        self.landed(name)
-        following = (kind, s + 1, d, ch)
-        if following in self.index:
-            self.start(following)
-        self.start(("p" + kind[0], s, d, ch))
-
-    def order(self):
-        names = []
-        for s in range(self.half_z):
-            if s == self.half_z // 2:
-                names += self.both("by", 0)
-            if s == self.half_z - 1:
-                names += self.both("by", 1)
-            names += self.both("az", s)
-        return names
-
-    def own_chip(self):
-        return [*self.both("pa", -1), *self.both("pb", -1)]
-
-    def handed(self):
-        return [n for n in self.index if n[0] in ("pa", "pb") and n[1] >= 0]
-
     def drain(self):
-        for name in self.index:
+        for name in self.tasks:
             self.copy(name).wait_send()
+
+
+def program_of(webs, delays):
+    times = foreseen({g: (web.tasks, web.sizes()) for g, web in webs.items()}, delays)
+    seen, begun, lines = set(), set(), []
+
+    def ready(group):
+        names = [
+            name
+            for name, (_, _, _, before) in webs[group].tasks.items()
+            if (group, name) not in begun and all((group, b) in seen for b in before)
+        ]
+        begun.update((group, name) for name in names)
+        return [(group, name) for name in names]
+
+    stops = [(delay, 0, group, None) for group, delay in delays.items()]
+    stops += [(time, 1, group, name) for (group, name), time in times.items()]
+    for time, _, group, name in sorted(stops, key=lambda s: (s[0], s[1], str(s[2:]))):
+        if name is not None:
+            seen.add((group, name))
+        lines.append((time, None if name is None else (group, name), ready(group)))
+    return lines, times
 
 
 MESH = pl.DeviceIdType.MESH
 CHUNK = 512
+W_DELAY = 18.0
+BLOCK_US = 1.0
 
 
 def layer_kernel(
@@ -324,11 +377,19 @@
     rows = rows_hbm.shape[0]
     share = rows // parts
     zs, ys, xs = ring_places(nz), ring_places(ny), ring_places(parts)
-    spread = Spread(held, sent, arrived, (z, y, core), *cuts)
-    w_spread = Spread(weights, w_sent, w_arrived, (z, y, core), *w_cuts)
+    place = (z, y, core, x, parts)
+    tasks, planes = copies_of(nz, ny, True)
+    w_tasks, w_planes = copies_of(nz, ny, False)
+    spread = Web(held, (sent, arrived), place, tasks, cuts, True)
+    w_spread = Web(weights, (w_sent, w_arrived), place, w_tasks, w_cuts, False)
+    webs = {"l": spread, "w": w_spread}
+    lines, times = program_of(webs, {"l": 0.0, "w": W_DELAY})
     model_rows = up_hbm.shape[0]
 
-    own_rows = pltpu.make_async_copy(rows_hbm, held.at[z, y, core], local_sem.at[0])
+    own_part = spread.rows("ab", spread.base)
+    own_rows = pltpu.make_async_copy(
+        rows_hbm.at[own_part], held.at[z, y, core, own_part], local_sem.at[0]
+    )
     own_rows.start()
     loads = [
         (up_hbm, weights.at[z, y, core, pl.ds(0, model_rows)]),
@@ -361,7 +422,15 @@
         pl.semaphore_signal(barrier, inc=1, device_id=neighbour, device_id_type=MESH)
     pl.semaphore_wait(barrier, len(neighbours))
     own_rows.wait()
-    spread.begin()
+
+    def carry_out(line):
+        _, landing, starts = line
+        if landing is not None:
+            webs[landing[0]].copy(landing[1]).wait_recv()
+        for group, name in starts:
+            webs[group].copy(name).start()
+
+    carry_out(lines.pop(0))
 
     def remote(src, dst, sems, i, device):
         return pltpu.make_async_remote_copy(
@@ -388,7 +457,6 @@
         copy.start()
     all_q_broad[core] = q_broad[...]
     all_q_narrow[core] = q_narrow[...]
-    spread.open_rings()
     for copy in exchange:
         copy.wait_recv()
     prepare(
@@ -403,53 +471,49 @@
         w_key,
         w_value_t,
     )
-    spread.landed(*spread.own_chip())
-    tools = (qt_broad, qt_narrow, w_key, w_value_t, top, total, acc)
-
-    def block_of(k):
-        return held[k // ny, lax.rem(k, ny)].reshape(2 * rows, -1)
-
-    attend_block(block_of(chip), True, *tools)
     for load in loads:
         load.wait()
-    for name in spread.order():
-        spread.pass_on(name)
-    w_spread.begin()
-    spread.landed(*spread.handed())
-
-    def opening():
-        w_spread.open_y()
-        w_spread.next_z(0)
-
-    def opened():
-        w_spread.open_z()
-        w_spread.next_z(1)
-
-    turns = {3: opening, 7: opened}
-    at = 10
-    for s in range(2, w_spread.half_z):
-        turns[at] = functools.partial(w_spread.next_z, s)
-        at += 3
-    w_order = w_spread.order()
-    early, late = w_order[:4], w_order[4:]
-    for i, name in enumerate(early):
-        turns[20 + i] = functools.partial(w_spread.pass_on, name)
-
-    def earlier(k, carried):
-        for turn, action in turns.items():
-            pl.when(k == turn)(action)
-
-        @pl.when(k < chip)
+    ready = [max(times["l", name] for name in planes[k]) for k in range(nz)]
+
+    def carry_out_until(time):
+        while lines and lines[0][0] <= time:
+            carry_out(lines.pop(0))
+
+    carry_out_until(ready[0])
+    tools = (qt_broad, qt_narrow, w_key, w_value_t, top, total, acc)
+
+    def block_of(at_z, at_y):
+        return held[at_z, at_y].reshape(2 * rows, -1)
+
+    attend_block(block_of(z, y), True, *tools)
+
+    turns, clock = {}, ready[0] + 1.2
+    for step in range(nz * ny):
+        clock = max(clock, ready[step // ny])
+        while lines and lines[0][0] <= clock:
+            turns.setdefault(step, []).append(lines.pop(0))
+        clock += BLOCK_US
+
+    def earlier(step, carried):
+        for turn, due in turns.items():
+
+            @pl.when(step == turn)
+            def _(due=due):
+                for line in due:
+                    carry_out(line)
+
+        k = step // ny
+        half = (k + 1) // 2
+        at_z = zs(z, half * (2 * lax.rem(k, 2) - 1))
+        at_y = lax.rem(step, ny)
+
+        @pl.when(at_z * ny + at_y < chip)
         def _():
-            attend_block(block_of(k), False, *tools)
+            attend_block(block_of(at_z, at_y), False, *tools)
 
         return carried
 
     lax.fori_loop(0, nz * ny, earlier, 0)
-
-    def more_turns(count):
-        for _ in range(min(count, len(late))):
-            w_spread.pass_on(late.pop(0))
 
     broad = jnp.transpose(acc[0:DB] / total[0])
     narrow = jnp.transpose(acc[DB : DB + DN] / total[1])
@@ -465,7 +529,7 @@
     for copy in to_owners:
         copy.start()
     gathered[pair] = finished[mine]
-    more_turns(4)
+    carry_out_until(clock + 2.0)
     for copy in to_owners:
         copy.wait_recv()
     rows_broad = jnp.concatenate([gathered[g, :, 0:DB] for g in range(2 * parts)], axis=1)
@@ -495,15 +559,15 @@
     ]
     around[0].start()
     around[1].start()
-    more_turns(4)
+    carry_out_until(clock + 10.0)
     around[0].wait_recv()
     around[2].start()
     around[1].wait_recv()
     around[3].start()
-    more_turns(len(late))
+    while lines:
+        carry_out(lines.pop(0))
     around[2].wait_recv()
     around[3].wait_recv()
-    w_spread.landed(*w_spread.own_chip(), *w_spread.handed())
     inputs = normed[...].reshape(rows, width)
 
     def raise_up(n, carried):
@@ -587,7 +651,8 @@
     model_rows = up_weight.shape[0]
     vmem = pl.BlockSpec(memory_space=pltpu.VMEM)
     anywhere = pl.BlockSpec(memory_space=pl.ANY)
-    copies = Spread.count(nz, ny)
+    copies = len(copies_of(nz, ny, True)[0])
+    w_copies = len(copies_of(nz, ny, False)[0])
     pieces = width // CHUNK
     sems = pltpu.SemaphoreType.DMA
     operands = (packed, *queries, *tables, *ups, *gains, resid, *outs, up_weight, down_weight)
@@ -626,8 +691,8 @@
             sems((6,)),
             sems((copies,)),
             sems((copies,)),
-            sems((copies,)),
-            sems((copies,)),
+            sems((w_copies,)),
+            sems((w_copies,)),
             sems((2,)),
             sems((2,)),
             sems((2 * parts - 1,)),
@@ -697,7 +762,7 @@
     cosines = jnp.concatenate([cosine, cosine], axis=0)
     sines = jnp.concatenate([-sine, sine], axis=0)
     return layer(
-        (nz, NY, parts, (80, 48, 64), (32, 16, 16)),
+        (nz, NY, parts, (32, 64, 16, 32), (32, 32, 16, 16)),
         packed,
         (query_broad, query_narrow),
         (cosines, sines),

time: 172 us -> 128 us (0.74)
  the two profiles are of different devices: /device:TPU:28 before, /device:TPU:232 now
where the time goes in v3:
time: 128 us; the launch traced here: 125 us
  Pallas kernels  118 us (92%)
  other arithmetic  4.31 us (3%)
  local copies, waits for them, and re-layouts  2.49 us (2%)
    pallas_call x1, Pallas kernels, layer(): pl.pallas_call(functools.partial(layer_kernel, geometry), out_shape=jax.S...  118 us

profile of v3, /device:TPU:232, one launch (start us, length us, event | category | flops | bytes accessed | tf_op | source)
XLA Modules:
  0.0 125.2 jit_solution(4574755976572500653)
XLA Ops:
  0.0 0.9 copy.19
  0.9 0.5 fusion.8
  1.4 1.0 fusion
  2.4 1.0 fusion.2
  3.5 0.8 pad_maximum_fusion.rows_hbm
  4.3 0.3 fusion.11
  4.6 0.7 pad_maximum_fusion.1
  5.3 118.4 %layer.1 = bf16[48,2048]{1,0:T(8,128)(2,1)} custom-call(bf16[192,640]{1,0:T(8,128)(2,1)} %pad_maximum_fusion.rows_hbm, bf16[192,384]{1,0:T(8,128)(2,1)} %q_broad.1, bf16[192,256]{1,0:T(8,128)(2,1)} %q_narrow.1, f32[64,384]{1,0:T(8,128)} %get-tuple-element.10.cosines, f32[64,384]{1,0:T(8,128)} %get-tuple-element.11.sines, bf16[512,256]{1,0:T(8,128)(2,1)} %key_up_broad.1, ...), custom_call_target="tpu_custom_call" | custom-call | flops 40000000000 | bytes 20000000 | tf_op jit(solution)/shard_map/layer/pallas_call | solution.py:659
  123.6 1.6 %copy.22 = bf16[48,2048]{1,0:T(8,128)(2,1)} copy(bf16[48,2048]{1,0:T(8,128)(2,1)} %layer.1) | data formatting | bytes 393216
  (7 shorter events, 0.1 us)

commit v4 on v3

--- a/solution.py
+++ b/solution.py
@@ -32,6 +32,7 @@
 
 
 LAST = ((1,), (1,))
+FIRST = ((0,), (0,))
 
 
 def prepare(core, q_broad, q_narrow, cosines, sines, refs, qt_broad, qt_narrow, w_key, w_value_t):
@@ -154,17 +155,40 @@
             tasks["by", k, 0, d] = (("y", d), "b", 1, column)
         tasks["by", k, 1, far] = (("y", far), "b", 1, (("by", k, 0, far),))
         plane += (("by", k, 0, 1), ("by", k, 0, -1), ("by", k, 1, far))
-        tasks["hand", k] = (("c", 0), "ab", ny, plane)
         if crossed:
-            for d in (1, -1):
-                tasks["x", k, d] = (("x", d), "ab", ny // 2, plane)
-            tasks["handx", k] = (("c", 0), "ab", ny, (("x", k, 1), ("x", k, -1)))
-            plane += (("x", k, 1), ("x", k, -1), ("handx", k))
-        planes[k] = plane + (("hand", k),)
+            tasks["hand", k] = (("c", 0), "ab", ny, plane)
+            given = (("hand", k),)
+        else:
+            round_y = ("ay", "az")
+            for rows in "ab":
+                parts = tuple(n for n in plane if (n[0] in round_y) == (rows == "a"))
+                tasks["hand" + rows, k] = (("c", 0), rows, ny, parts)
+            given = (("handa", k), ("handb", k))
+        if crossed:
+            if k == 0:
+                blocks = (
+                    (),
+                    (("ay", 0, 1), ("by", 0, 0, 1)),
+                    (("ay", 0, -1), ("by", 0, 0, -1)),
+                    (("ay", 1, 1), ("ay", 1, -1), ("by", 0, 1, far)),
+                )
+                pieces = []
+                for j, before in enumerate(blocks):
+                    for d in (1, -1):
+                        tasks["x0", j, d] = (("x", d), "x" + "+-"[d < 0] + "eo"[j % 2], 1, before)
+                        pieces.append(("x0", j, d))
+            else:
+                pieces = [("x", k, 1), ("x", k, -1)]
+                for d in (1, -1):
+                    tasks["x", k, d] = (("x", d), "x", ny // 2, plane)
+            pieces = tuple(pieces)
+            tasks["handx", k] = (("c", 0), "x", ny, pieces)
+            plane += (*pieces, ("handx", k))
+        planes[k] = plane + given
     return tasks, planes
 
 
-def foreseen(groups, delays, link_rate=46.0, chip_rate=450.0, latency=2.0):
+def foreseen(groups, delays, link_rate=43.5, chip_rate=450.0, latency=2.2):
     landed, waiting, free, now = {}, set(), {}, 0.0
     pending = []
     for g, (tasks, sizes) in groups.items():
@@ -221,6 +245,11 @@
             "b+": (a, b_cut),
             "b-": (a + b_cut, b - b_cut),
             "ab": (0, a + b),
+            "x": (0, a + b),
+            "x+e": (0, (a + b) // 2),
+            "x-e": ((a + b) // 2, (a + b) // 2),
+            "x+o": (0, (a + b) // 2),
+            "x-o": ((a + b) // 2, (a + b) // 2),
         }
         parity = lax.rem(self.x, 2) if crossed else 0
         self.base = parity * (a + b)
@@ -253,6 +282,8 @@
             at = (zs(z, -name[1] * name[2]), y)
         elif kind == "by":
             at = (zs(z, offset_of(name[1])), ys(y, -name[2] * name[3]))
+        elif kind == "x0":
+            at = (z, ys(y, Y_BLOCKS[name[1]]))
         elif kind == "x":
             half = self.ny // 2
             at = (zs(z, offset_of(name[1])), pl.ds(0 if name[2] == 1 else half, half))
@@ -305,17 +336,22 @@
 
 MESH = pl.DeviceIdType.MESH
 CHUNK = 512
-W_DELAY = 18.0
-BLOCK_US = 1.0
+W_DELAY = 16.0
+BLOCK_US = 1.6
+LAG_US = 0.0
 
 
 def layer_kernel(
     geometry,
-    rows_hbm,
+    latent_hbm,
     q_broad,
     q_narrow,
     cosines,
     sines,
+    key_cosines,
+    key_sines,
+    key_rope,
+    latent_gain,
     key_up_broad,
     value_up_broad,
     key_up_narrow,
@@ -340,7 +376,12 @@
     top,
     total,
     acc,
-    finished,
+    latent,
+    rotated,
+    broad_done,
+    narrow_done,
+    broad_theirs,
+    narrow_theirs,
     gathered,
     out_broad,
     out_narrow,
@@ -374,7 +415,7 @@
     core = lax.rem(me, 2)
     chip = me // 2
     z, y = chip // ny, lax.rem(chip, ny)
-    rows = rows_hbm.shape[0]
+    rows = latent_hbm.shape[0]
     share = rows // parts
     zs, ys, xs = ring_places(nz), ring_places(ny), ring_places(parts)
     place = (z, y, core, x, parts)
@@ -387,16 +428,14 @@
     model_rows = up_hbm.shape[0]
 
     own_part = spread.rows("ab", spread.base)
-    own_rows = pltpu.make_async_copy(
-        rows_hbm.at[own_part], held.at[z, y, core, own_part], local_sem.at[0]
-    )
+    own_rows = pltpu.make_async_copy(latent_hbm.at[own_part], latent, local_sem.at[0])
     own_rows.start()
     loads = [
         (up_hbm, weights.at[z, y, core, pl.ds(0, model_rows)]),
         (down_hbm, weights.at[z, y, core, pl.ds(model_rows, model_rows)]),
         (out_broad_hbm, out_broad),
         (out_narrow_hbm, out_narrow),
-        (resid_hbm.at[pl.ds(x * share, share)], resid),
+        (resid_hbm, resid),
     ]
     loads = [
         pltpu.make_async_copy(src, dst, local_sem.at[i + 1]) for i, (src, dst) in enumerate(loads)
@@ -404,24 +443,37 @@
     for load in loads:
         load.start()
 
-    def tile_peer(offset):
-        there = lax.rem(core * parts + x + offset, 2 * parts)
-        return there, {
-            "sp": (z * ny + y) * 2 + there // parts,
-            "tp": lax.rem(there, parts),
-        }
-
+    right, left = {"tp": xs(x, 1)}, {"tp": xs(x, -1)}
     barrier = pltpu.get_barrier_semaphore()
-    neighbours = [tile_peer(offset)[1] for offset in range(1, 2 * parts)] + [
+    neighbours = [
+        spread.device(z, y, 1 - core),
         spread.device(z, ys(y, 1), core),
         spread.device(z, ys(y, -1), core),
         spread.device(zs(z, 1), y, core),
         spread.device(zs(z, -1), y, core),
+        right,
+        left,
     ]
     for neighbour in neighbours:
         pl.semaphore_signal(barrier, inc=1, device_id=neighbour, device_id_type=MESH)
+
+    tail = latent.shape[1]
+    straight = dot(key_rope[...], picker((ROPE, 128), lambda r, k: r == k - ROPE), FIRST)
+    swapped = dot(
+        key_rope[...],
+        picker(
+            (ROPE, 128),
+            lambda r, k: (k >= ROPE) & (r == jnp.where(k < ROPE + 32, k - 32, k - ROPE - 32)),
+        ),
+        FIRST,
+    )
+    rotated[...] = (straight * key_cosines[...] + swapped * key_sines[...]).astype(bf16)
+    held[z, y, core, own_part, tail : tail + 128] = rotated[own_part, :]
+    own_rows.wait()
+    held[z, y, core, own_part, 0:tail] = rms_scale(latent[...].astype(f32), latent_gain[...]).astype(
+        bf16
+    )
     pl.semaphore_wait(barrier, len(neighbours))
-    own_rows.wait()
 
     def carry_out(line):
         _, landing, starts = line
@@ -487,10 +539,16 @@
 
     attend_block(block_of(z, y), True, *tools)
 
-    turns, clock = {}, ready[0] + 1.2
-    for step in range(nz * ny):
-        clock = max(clock, ready[step // ny])
-        while lines and lines[0][0] <= clock:
+    @pl.when(lax.rem(y, 2) == 1)
+    def _():
+        attend_block(block_of(z, y - 1), False, *tools)
+
+
+    turns, clock = {}, ready[0] + 2.0
+    steps = nz * ny // 2
+    for step in range(steps):
+        clock = max(clock, ready[step // (ny // 2)])
+        while lines and lines[0][0] <= clock + LAG_US:
             turns.setdefault(step, []).append(lines.pop(0))
         clock += BLOCK_US
 
@@ -502,38 +560,74 @@
                 for line in due:
                     carry_out(line)
 
-        k = step // ny
+        k = step // (ny // 2)
         half = (k + 1) // 2
         at_z = zs(z, half * (2 * lax.rem(k, 2) - 1))
-        at_y = lax.rem(step, ny)
-
-        @pl.when(at_z * ny + at_y < chip)
+        at_y = 2 * lax.rem(step, ny // 2)
+
+        @pl.when(at_z * ny + at_y + 1 < chip)
         def _():
-            attend_block(block_of(at_z, at_y), False, *tools)
+            attend_block(held[at_z, pl.ds(at_y, 2)].reshape(4 * rows, -1), False, *tools)
 
         return carried
 
-    lax.fori_loop(0, nz * ny, earlier, 0)
-
-    broad = jnp.transpose(acc[0:DB] / total[0])
-    narrow = jnp.transpose(acc[DB : DB + DN] / total[1])
-    finished[...] = (
-        jnp.concatenate([broad, narrow], axis=1).astype(bf16).reshape(2 * parts, share, DB + DN)
-    )
-    mine = core * parts + x
-    pair = 2 * x + core
-    to_owners = []
-    for offset in range(1, 2 * parts):
-        there, device = tile_peer(offset)
-        to_owners.append(remote(finished.at[there], gathered.at[pair], a_sems, offset - 1, device))
-    for copy in to_owners:
+    lax.fori_loop(0, steps, earlier, 0)
+
+    broad_done[...] = jnp.transpose(acc[0:DB] / total[0]).astype(bf16).reshape(2, rows, DB)
+    narrow_done[...] = (
+        jnp.transpose(acc[DB : DB + DN] / total[1]).astype(bf16).reshape(2, rows, DN)
+    )
+    swap = [
+        remote(broad_done.at[1 - core], broad_theirs, a_sems, 0, partner),
+        remote(narrow_done.at[1 - core], narrow_theirs, a_sems, 1, partner),
+    ]
+    for copy in swap:
         copy.start()
-    gathered[pair] = finished[mine]
-    carry_out_until(clock + 2.0)
-    for copy in to_owners:
+    carry_out_until(clock + 1.5)
+    for copy in swap:
         copy.wait_recv()
-    rows_broad = jnp.concatenate([gathered[g, :, 0:DB] for g in range(2 * parts)], axis=1)
-    rows_narrow = jnp.concatenate([gathered[g, :, DB : DB + DN] for g in range(2 * parts)], axis=1)
+    pairs = [
+        (mine, theirs[...])
+        for mine, theirs in (
+            (broad_done[core], broad_theirs),
+            (narrow_done[core], narrow_theirs),
+        )
+    ]
+    gathered[x] = jnp.concatenate(
+        [half for mine, theirs in pairs for half in (
+            jnp.where(core == 0, mine, theirs), jnp.where(core == 0, theirs, mine)
+        )],
+        axis=1,
+    )
+    halves = (pl.ds(0, rows // 2), pl.ds(rows // 2, rows // 2))
+
+    def along_x(at, half, i, device):
+        view = gathered.at[at, halves[half]]
+        return remote(view, view, n_sems, i, device)
+
+    around = [
+        along_x(x, 0, 0, right),
+        along_x(x, 1, 1, left),
+        along_x(x, 1, 2, right),
+        along_x(x, 0, 3, left),
+        along_x(xs(x, -1), 0, 4, right),
+        along_x(xs(x, 1), 1, 5, left),
+    ]
+    for copy in around[:4]:
+        copy.start()
+    spread.drain()
+    carry_out_until(clock + 5.0)
+    around[0].wait_recv()
+    around[4].start()
+    around[1].wait_recv()
+    around[5].start()
+    carry_out_until(clock + 9.0)
+    for copy in around[2:]:
+        copy.wait_recv()
+    rows_broad = jnp.concatenate([gathered[i, :, 0 : 2 * DB] for i in range(parts)], axis=1)
+    rows_narrow = jnp.concatenate(
+        [gathered[i, :, 2 * DB : 2 * (DB + DN)] for i in range(parts)], axis=1
+    )
     width = out.shape[1]
 
     def project(n, carried):
@@ -544,31 +638,19 @@
         return carried
 
     lax.fori_loop(0, width // CHUNK, project, 0)
-    mix = (resid[...].astype(f32) + rms_scale(wide[...], post_gain[...])).astype(bf16)
-    mixed[...] = mix
-    normed[x] = rms_scale(mix.astype(f32), ffn_gain[...]).astype(bf16)
-    right, left = {"tp": xs(x, 1)}, {"tp": xs(x, -1)}
-    first_rows, last_rows = pl.ds(0, 32), pl.ds(32, share - 32)
-    around = [
-        remote(normed.at[x], normed.at[x], n_sems, 0, right),
-        remote(normed.at[x], normed.at[x], n_sems, 1, left),
-        remote(
-            normed.at[xs(x, -1), first_rows], normed.at[xs(x, -1), first_rows], n_sems, 2, right
-        ),
-        remote(normed.at[xs(x, 1), last_rows], normed.at[xs(x, 1), last_rows], n_sems, 3, left),
-    ]
-    around[0].start()
-    around[1].start()
-    carry_out_until(clock + 10.0)
-    around[0].wait_recv()
-    around[2].start()
-    around[1].wait_recv()
-    around[3].start()
-    while lines:
-        carry_out(lines.pop(0))
-    around[2].wait_recv()
-    around[3].wait_recv()
+
+    def norm_share(i, carried):
+        at = pl.ds(pl.multiple_of(i * share, 16), share)
+        mix = (resid[at].astype(f32) + rms_scale(wide[at], post_gain[...])).astype(bf16)
+        mixed[i] = mix
+        normed[i] = rms_scale(mix.astype(f32), ffn_gain[...]).astype(bf16)
+        return carried
+
+    lax.fori_loop(0, parts, norm_share, 0)
     inputs = normed[...].reshape(rows, width)
+    carry_out_until(
+        max(times["w", n] for k in range(nz) for n in w_planes[k] if n[0] in ("ay", "az", "handa"))
+    )
 
     def raise_up(n, carried):
         columns = pl.ds(pl.multiple_of(n * CHUNK, CHUNK), CHUNK)
@@ -578,6 +660,8 @@
         return carried
 
     lax.fori_loop(0, hidden.shape[1] // CHUNK, raise_up, 0)
+    while lines:
+        carry_out(lines.pop(0))
 
     pieces = width // CHUNK
     per_z = 2 * ny * model_rows
@@ -619,18 +703,16 @@
 
     for n in range(pieces):
         lower(n)
-        if n > 0:
-            relay(n - 1)
-    relay(pieces - 1)
+    for n in range(pieces):
+        relay(n)
+    w_spread.drain()
+    for copy in exchange + swap + around:
+        copy.wait_send()
     for n in range(pieces):
         copies[n][1].wait_recv()
         copies[n][2].wait_recv()
     ffn = partial[x] + from_near[...].astype(f32) + from_far[...].astype(f32)
-    out[...] = (mixed[...].astype(f32) + rms_scale(ffn, ffn_out_gain[...])).astype(bf16)
-    spread.drain()
-    w_spread.drain()
-    for copy in exchange + to_owners + around:
-        copy.wait_send()
+    out[...] = (mixed[x].astype(f32) + rms_scale(ffn, ffn_out_gain[...])).astype(bf16)
     for n in range(pieces):
         for copy in copies[n]:
             copy.wait_send()
@@ -642,9 +724,9 @@
     )
 
 
-def layer(geometry, packed, queries, tables, ups, gains, resid, outs, up_weight, down_weight):
+def layer(geometry, latent, queries, tables, key_rope, ups, gains, resid, outs, up_weight, down_weight):
     nz, ny, parts = geometry[:3]
-    rows, latent_width = packed.shape
+    rows, latent_width = latent.shape
     width = resid.shape[1]
     hidden = up_weight.shape[1]
     share = rows // parts
@@ -655,14 +737,26 @@
     w_copies = len(copies_of(nz, ny, False)[0])
     pieces = width // CHUNK
     sems = pltpu.SemaphoreType.DMA
-    operands = (packed, *queries, *tables, *ups, *gains, resid, *outs, up_weight, down_weight)
+    operands = (
+        latent,
+        *queries,
+        *tables,
+        key_rope,
+        gains[0],
+        *ups,
+        *gains[1:],
+        resid,
+        *outs,
+        up_weight,
+        down_weight,
+    )
     return pl.pallas_call(
         functools.partial(layer_kernel, geometry),
         out_shape=jax.ShapeDtypeStruct((share, width), bf16),
-        in_specs=[anywhere] + [vmem] * 11 + [anywhere] * 5,
+        in_specs=[anywhere] + [vmem] * 15 + [anywhere] * 5,
         out_specs=vmem,
         scratch_shapes=[
-            pltpu.VMEM((nz, ny, 2, rows, latent_width), bf16),
+            pltpu.VMEM((nz, ny, 2, rows, latent_width + 128), bf16),
             pltpu.VMEM((nz, ny, 2, 2 * model_rows, hidden), bf16),
             pltpu.VMEM((2, rows, queries[0].shape[1]), bf16),
             pltpu.VMEM((2, rows, queries[1].shape[1]), bf16),
@@ -673,13 +767,18 @@
             pltpu.VMEM((2, 1, 2 * rows), f32),
             pltpu.VMEM((2, 1, 2 * rows), f32),
             pltpu.VMEM((DB + DN, 2 * rows), f32),
-            pltpu.VMEM((2 * parts, share, DB + DN), bf16),
-            pltpu.VMEM((2 * parts, share, DB + DN), bf16),
+            pltpu.VMEM((rows // 2, latent_width), bf16),
+            pltpu.VMEM((rows, 128), bf16),
+            pltpu.VMEM((2, rows, DB), bf16),
+            pltpu.VMEM((2, rows, DN), bf16),
+            pltpu.VMEM((rows, DB), bf16),
+            pltpu.VMEM((rows, DN), bf16),
+            pltpu.VMEM((parts, rows, 2 * (DB + DN)), bf16),
             pltpu.VMEM(outs[0].shape, bf16),
             pltpu.VMEM(outs[1].shape, bf16),
-            pltpu.VMEM((share, width), bf16),
-            pltpu.VMEM((share, width), f32),
-            pltpu.VMEM((share, width), bf16),
+            pltpu.VMEM((rows, width), bf16),
+            pltpu.VMEM((rows, width), f32),
+            pltpu.VMEM((parts, share, width), bf16),
             pltpu.VMEM((parts, share, width), bf16),
             pltpu.VMEM((rows, hidden), bf16),
             pltpu.VMEM((parts, share, width), f32),
@@ -695,10 +794,10 @@
             sems((w_copies,)),
             sems((2,)),
             sems((2,)),
-            sems((2 * parts - 1,)),
-            sems((2 * parts - 1,)),
-            sems((4,)),
-            sems((4,)),
+            sems((2,)),
+            sems((2,)),
+            sems((6,)),
+            sems((6,)),
             sems((3 * pieces,)),
             sems((3 * pieces,)),
         ],
@@ -712,10 +811,8 @@
     )(*operands)
 
 
-def angles_of(first, count):
-    frequency = rope_base ** (-2.0 * jnp.arange(ROPE // 2, dtype=f32) / ROPE)
-    positions = (first + jnp.arange(count, dtype=jnp.int32)).astype(f32)
-    return positions, frequency
+def frequency_of(lane):
+    return rope_base ** (-2.0 * lax.rem(lane, ROPE // 2).astype(f32) / ROPE)
 
 
 def local(
@@ -742,32 +839,25 @@
     me = lax.axis_index("sp")
     nz = lax.axis_size("sp") // (2 * NY)
 
-    positions, frequency = angles_of(me * rows, rows)
-    angles = positions[:, None] * frequency[None, :]
-    cosine, sine = jnp.cos(angles), jnp.sin(angles)
-    leading, trailing = jnp.split(key_rope.astype(f32), 2, axis=1)
-    latent_normed = rms_scale(latent.astype(f32), latent_gain).astype(bf16)
-    packed = jnp.concatenate(
-        [
-            latent_normed,
-            jnp.zeros((rows, 64), bf16),
-            (leading * cosine - trailing * sine).astype(bf16),
-            (trailing * cosine + leading * sine).astype(bf16),
-        ],
-        axis=1,
-    )
-    positions, frequency = angles_of((me // 2) * 2 * rows, 2 * rows)
-    angles = frequency[:, None] * positions[None, :]
-    cosine, sine = jnp.cos(angles), jnp.sin(angles)
-    cosines = jnp.concatenate([cosine, cosine], axis=0)
-    sines = jnp.concatenate([-sine, sine], axis=0)
+    lane = jnp.arange(128, dtype=jnp.int32)
+    positions = (me * rows + jnp.arange(rows, dtype=jnp.int32)).astype(f32)
+    angles = positions[:, None] * frequency_of(lane)[None, :]
+    sign = jnp.where(lane < ROPE, 0.0, jnp.where(lane < ROPE + ROPE // 2, -1.0, 1.0))
+    key_cosines = jnp.cos(angles) * (sign * sign)[None, :]
+    key_sines = jnp.sin(angles) * sign[None, :]
+    lane = jnp.arange(ROPE, dtype=jnp.int32)
+    positions = ((me // 2) * 2 * rows + jnp.arange(2 * rows, dtype=jnp.int32)).astype(f32)
+    angles = frequency_of(lane)[:, None] * positions[None, :]
+    cosines = jnp.cos(angles)
+    sines = jnp.sin(angles) * jnp.where(lane < ROPE // 2, -1.0, 1.0)[:, None]
     return layer(
         (nz, NY, parts, (32, 64, 16, 32), (32, 32, 16, 16)),
-        packed,
+        latent,
         (query_broad, query_narrow),
-        (cosines, sines),
+        (cosines, sines, key_cosines, key_sines),
+        key_rope.T,
         (key_up_broad, value_up_broad, key_up_narrow, value_up_narrow),
-        (post_gain[None, :], ffn_gain[None, :], ffn_out_gain[None, :]),
+        (latent_gain[None, :], post_gain[None, :], ffn_gain[None, :], ffn_out_gain[None, :]),
         resid,
         (out_broad, out_narrow),
         up_weight,

time: 128 us -> 110 us (0.86)
  the two profiles are of different devices: /device:TPU:232 before, /device:TPU:96 now
where the time goes in v4:
time: 110 us
  Pallas kernels  106 us (96%)
  other arithmetic  2.23 us (2%)
  local copies, waits for them, and re-layouts  1.62 us (1%)
    pallas_call x1, Pallas kernels, layer(): pl.pallas_call(functools.partial(layer_kernel, geometry), out_shape=jax.S...  106 us

profile of v4, /device:TPU:96, one launch (start us, length us, event | category | flops | bytes accessed | tf_op | source)
XLA Modules:
  0.0 109.6 jit_solution(17368124216321450583)
XLA Ops:
  0.1 1.1 %fusion = (f32[64,384]{1,0:T(8,128)}, f32[64,384]{1,0:T(8,128)}) fusion(f32[64]{0:T(128)S(1)} %get-tuple-element.9, f32[384]{0:T(512)S(1)} %add_convert_fusion, f32[64]{0:T(128)S(1)} %get-tuple-element.10), kind=kLoop, calls=%fused_computation.4 | loop fusion | flops 49152 | bytes 198656 | tf_op jit(solution)/shard_map/mul | solution.py:852
  1.2 1.1 fusion.2
  2.3 105.7 %layer.1 = bf16[48,2048]{1,0:T(8,128)(2,1)} custom-call(bf16[192,512]{1,0:T(8,128)(2,1)} %latent_hbm.1, bf16[192,384]{1,0:T(8,128)(2,1)} %q_broad.1, bf16[192,256]{1,0:T(8,128)(2,1)} %q_narrow.1, f32[64,384]{1,0:T(8,128)} %get-tuple-element.6.cosines, f32[64,384]{1,0:T(8,128)} %get-tuple-element.5.sines, f32[192,128]{1,0:T(8,128)} %get-tuple-element.8.key_cosines, ...), custom_call_target="tpu_custom_call" | custom-call | flops 40000000000 | bytes 20000000 | tf_op jit(solution)/shard_map/layer/pallas_call | solution.py:753
  108.0 1.6 %copy.19 = bf16[48,2048]{1,0:T(8,128)(2,1)} copy(bf16[48,2048]{1,0:T(8,128)(2,1)} %layer.1) | data formatting | bytes 393216
  (5 shorter events, 0.0 us)

commit v5 on v4

--- a/solution.py
+++ b/solution.py
@@ -155,15 +155,7 @@
             tasks["by", k, 0, d] = (("y", d), "b", 1, column)
         tasks["by", k, 1, far] = (("y", far), "b", 1, (("by", k, 0, far),))
         plane += (("by", k, 0, 1), ("by", k, 0, -1), ("by", k, 1, far))
-        if crossed:
-            tasks["hand", k] = (("c", 0), "ab", ny, plane)
-            given = (("hand", k),)
-        else:
-            round_y = ("ay", "az")
-            for rows in "ab":
-                parts = tuple(n for n in plane if (n[0] in round_y) == (rows == "a"))
-                tasks["hand" + rows, k] = (("c", 0), rows, ny, parts)
-            given = (("handa", k), ("handb", k))
+        tasks["hand", k] = (("c", 0), "ab", ny, plane)
         if crossed:
             if k == 0:
                 blocks = (
@@ -184,7 +176,7 @@
             pieces = tuple(pieces)
             tasks["handx", k] = (("c", 0), "x", ny, pieces)
             plane += (*pieces, ("handx", k))
-        planes[k] = plane + given
+        planes[k] = plane + (("hand", k),)
     return tasks, planes
 
 
@@ -230,40 +222,29 @@
 
 
 class Web:
-    def __init__(self, held, sems, place, tasks, cuts, crossed):
+    def __init__(self, held, sems, place, tasks, spans, crossed):
         self.held, self.sent, self.arrived = held, *sems
         self.z, self.y, self.core, self.x, self.parts = place
         self.nz, self.ny = held.shape[:2]
         self.tasks = tasks
         self.index = {name: i for i, name in enumerate(tasks)}
-        a, b, a_cut, b_cut = cuts
-        self.spans = {
-            "a": (0, a),
-            "b": (a, b),
-            "a+": (0, a_cut),
-            "a-": (a_cut, a - a_cut),
-            "b+": (a, b_cut),
-            "b-": (a + b_cut, b - b_cut),
-            "ab": (0, a + b),
-            "x": (0, a + b),
-            "x+e": (0, (a + b) // 2),
-            "x-e": ((a + b) // 2, (a + b) // 2),
-            "x+o": (0, (a + b) // 2),
-            "x-o": ((a + b) // 2, (a + b) // 2),
+        self.spans = spans
+        self.count = spans["ab"][1]
+        parity = lax.rem(self.x, 2) if crossed else 0
+        self.base = parity * self.count
+        self.other_base = (1 - parity) * self.count
+
+    def sizes(self):
+        return {
+            key: rows * columns * 2 * (rows > 0) for key, (_, rows, _, columns) in self.spans.items()
         }
-        parity = lax.rem(self.x, 2) if crossed else 0
-        self.base = parity * (a + b)
-        self.other_base = (1 - parity) * (a + b)
-
-    def sizes(self):
-        row = self.held.shape[4] * 2
-        return {key: size * row for key, (_, size) in self.spans.items()}
-
-    def rows(self, key, base):
-        start, size = self.spans[key]
-        if isinstance(base, int):
-            return pl.ds(base + start, size)
-        return pl.ds(pl.multiple_of(base + start, 16), size)
+
+    def part(self, key, base):
+        start, rows, first, columns = self.spans[key]
+        at = base + start
+        if not isinstance(base, int):
+            at = pl.multiple_of(at, 16)
+        return pl.ds(at, rows), pl.ds(first, columns)
 
     def device(self, z, y, core):
         return {"sp": (z * self.ny + y) * 2 + core}
@@ -273,7 +254,7 @@
         link, key, _, _ = self.tasks[name]
         zs, ys, xs = ring_places(self.nz), ring_places(self.ny), ring_places(self.parts)
         z, y, c = self.z, self.y, self.core
-        rows = self.rows(key, self.other_base if kind == "handx" else self.base)
+        rows, columns = self.part(key, self.other_base if kind == "handx" else self.base)
         if kind == "ay":
             at = (z, ys(y, -name[1] * name[2]))
         elif kind == "az":
@@ -289,7 +270,7 @@
             at = (zs(z, offset_of(name[1])), pl.ds(0 if name[2] == 1 else half, half))
         else:
             at = (zs(z, offset_of(name[1])), pl.ds(0, self.ny))
-        view = self.held.at[at[0], at[1], c, rows]
+        view = self.held.at[at[0], at[1], c, rows, columns]
         axis, d = link
         to = {
             "y": lambda: self.device(z, ys(y, d), c),
@@ -312,6 +293,35 @@
             self.copy(name).wait_send()
 
 
+def split_rows(a, b, a_cut, b_cut, columns):
+    half = (a + b) // 2
+    rows = {
+        "a": (0, a),
+        "b": (a, b),
+        "a+": (0, a_cut),
+        "a-": (a_cut, a - a_cut),
+        "b+": (a, b_cut),
+        "b-": (a + b_cut, b - b_cut),
+        "ab": (0, a + b),
+        "x": (0, a + b),
+        "x+e": (0, half),
+        "x-e": (half, half),
+        "x+o": (0, half),
+        "x-o": (half, half),
+    }
+    return {key: (*span, 0, columns) for key, span in rows.items()}
+
+
+def split_columns(rows, cut, columns):
+    half = rows // 2
+    spans = {"ab": (0, rows, 0, columns)}
+    for key, first, size in (("a", 0, cut), ("b", cut, columns - cut)):
+        spans[key] = (0, rows, first, size)
+        spans[key + "+"] = (0, half, first, size)
+        spans[key + "-"] = (half, half, first, size)
+    return spans
+
+
 def program_of(webs, delays):
     times = foreseen({g: (web.tasks, web.sizes()) for g, web in webs.items()}, delays)
     seen, begun, lines = set(), set(), []
@@ -336,7 +346,10 @@
 
 MESH = pl.DeviceIdType.MESH
 CHUNK = 512
-W_DELAY = 16.0
+UP_DELAY = 10.0
+DOWN_DELAY = 20.0
+W_CUT = 896
+L_CUTS = (32, 64, 16, 32)
 BLOCK_US = 1.6
 LAG_US = 0.0
 
@@ -366,7 +379,8 @@
     down_hbm,
     out,
     held,
-    weights,
+    up_held,
+    down_held,
     all_q_broad,
     all_q_narrow,
     qt_broad,
@@ -399,8 +413,10 @@
     local_sem,
     sent,
     arrived,
-    w_sent,
-    w_arrived,
+    up_sent,
+    up_arrived,
+    down_sent,
+    down_arrived,
     q_sent,
     q_arrived,
     a_sent,
@@ -410,7 +426,7 @@
     r_sent,
     r_arrived,
 ):
-    nz, ny, parts, cuts, w_cuts = geometry
+    nz, ny, parts = geometry
     me, x = lax.axis_index("sp"), lax.axis_index("tp")
     core = lax.rem(me, 2)
     chip = me // 2
@@ -421,18 +437,20 @@
     place = (z, y, core, x, parts)
     tasks, planes = copies_of(nz, ny, True)
     w_tasks, w_planes = copies_of(nz, ny, False)
-    spread = Web(held, (sent, arrived), place, tasks, cuts, True)
-    w_spread = Web(weights, (w_sent, w_arrived), place, w_tasks, w_cuts, False)
-    webs = {"l": spread, "w": w_spread}
-    lines, times = program_of(webs, {"l": 0.0, "w": W_DELAY})
-    model_rows = up_hbm.shape[0]
-
-    own_part = spread.rows("ab", spread.base)
+    model_rows, w_columns = up_hbm.shape
+    w_spans = split_columns(model_rows, W_CUT, w_columns)
+    spread = Web(held, (sent, arrived), place, tasks, split_rows(*L_CUTS, held.shape[4]), True)
+    up_web = Web(up_held, (up_sent, up_arrived), place, w_tasks, w_spans, False)
+    down_web = Web(down_held, (down_sent, down_arrived), place, w_tasks, w_spans, False)
+    webs = {"l": spread, "u": up_web, "w": down_web}
+    lines, times = program_of(webs, {"l": 0.0, "u": UP_DELAY, "w": DOWN_DELAY})
+
+    own_part, _ = spread.part("ab", spread.base)
     own_rows = pltpu.make_async_copy(latent_hbm.at[own_part], latent, local_sem.at[0])
     own_rows.start()
     loads = [
-        (up_hbm, weights.at[z, y, core, pl.ds(0, model_rows)]),
-        (down_hbm, weights.at[z, y, core, pl.ds(model_rows, model_rows)]),
+        (up_hbm, up_held.at[z, y, core]),
+        (down_hbm, down_held.at[z, y, core]),
         (out_broad_hbm, out_broad),
         (out_narrow_hbm, out_narrow),
         (resid_hbm, resid),
@@ -648,13 +666,11 @@
 
     lax.fori_loop(0, parts, norm_share, 0)
     inputs = normed[...].reshape(rows, width)
-    carry_out_until(
-        max(times["w", n] for k in range(nz) for n in w_planes[k] if n[0] in ("ay", "az", "handa"))
-    )
+    carry_out_until(max(times["u", name] for name in w_tasks))
 
     def raise_up(n, carried):
         columns = pl.ds(pl.multiple_of(n * CHUNK, CHUNK), CHUNK)
-        up = weights[:, :, :, 0:model_rows, columns].reshape(width, CHUNK)
+        up = up_held[:, :, :, :, columns].reshape(width, CHUNK)
         raised = jnp.maximum(dot(inputs, up), 0.0)
         hidden[:, columns] = (raised * raised).astype(bf16)
         return carried
@@ -685,9 +701,7 @@
     def lower(n):
         columns = slice(n * CHUNK, (n + 1) * CHUNK)
         zn = CHUNK // per_z
-        down = weights[n * zn : (n + 1) * zn, :, :, model_rows : 2 * model_rows].reshape(
-            CHUNK, hidden.shape[1]
-        )
+        down = down_held[n * zn : (n + 1) * zn].reshape(CHUNK, hidden.shape[1])
         sums = dot(hidden[...], down, LAST).reshape(parts, share, CHUNK)
         partial[:, :, columns] = sums
         partial_sent[:, :, columns] = sums.astype(bf16)
@@ -705,7 +719,8 @@
         lower(n)
     for n in range(pieces):
         relay(n)
-    w_spread.drain()
+    up_web.drain()
+    down_web.drain()
     for copy in exchange + swap + around:
         copy.wait_send()
     for n in range(pieces):
@@ -725,7 +740,7 @@
 
 
 def layer(geometry, latent, queries, tables, key_rope, ups, gains, resid, outs, up_weight, down_weight):
-    nz, ny, parts = geometry[:3]
+    nz, ny, parts = geometry
     rows, latent_width = latent.shape
     width = resid.shape[1]
     hidden = up_weight.shape[1]
@@ -757,7 +772,8 @@
         out_specs=vmem,
         scratch_shapes=[
             pltpu.VMEM((nz, ny, 2, rows, latent_width + 128), bf16),
-            pltpu.VMEM((nz, ny, 2, 2 * model_rows, hidden), bf16),
+            pltpu.VMEM((nz, ny, 2, model_rows, hidden), bf16),
+            pltpu.VMEM((nz, ny, 2, model_rows, hidden), bf16),
             pltpu.VMEM((2, rows, queries[0].shape[1]), bf16),
             pltpu.VMEM((2, rows, queries[1].shape[1]), bf16),
             pltpu.VMEM((256, 2 * rows), bf16),
@@ -792,6 +808,8 @@
             sems((copies,)),
             sems((w_copies,)),
             sems((w_copies,)),
+            sems((w_copies,)),
+            sems((w_copies,)),
             sems((2,)),
             sems((2,)),
             sems((2,)),
@@ -851,7 +869,7 @@
     cosines = jnp.cos(angles)
     sines = jnp.sin(angles) * jnp.where(lane < ROPE // 2, -1.0, 1.0)[:, None]
     return layer(
-        (nz, NY, parts, (32, 64, 16, 32), (32, 32, 16, 16)),
+        (nz, NY, parts),
         latent,
         (query_broad, query_narrow),
         (cosines, sines, key_cosines, key_sines),

time: 110 us -> 109 us (level)
  the two profiles are of different devices: /device:TPU:96 before, /device:TPU:20 now
where the time goes in v5:
time: 109 us
  Pallas kernels  105 us (96%)
  other arithmetic  2.23 us (2%)
  local copies, waits for them, and re-layouts  1.62 us (1%)
    pallas_call x1, Pallas kernels, layer(): pl.pallas_call(functools.partial(layer_kernel, geometry), out_shape=jax.S...  105 us

profile of v5, /device:TPU:20, one launch (start us, length us, event | category | flops | bytes accessed | tf_op | source)
XLA Modules:
  0.0 109.1 jit_solution(9277999312711100649)
XLA Ops:
  0.1 1.1 %fusion = (f32[64,384]{1,0:T(8,128)}, f32[64,384]{1,0:T(8,128)}) fusion(f32[64]{0:T(128)S(1)} %get-tuple-element.9, f32[384]{0:T(512)S(1)} %add_convert_fusion, f32[64]{0:T(128)S(1)} %get-tuple-element.10), kind=kLoop, calls=%fused_computation.4 | loop fusion | flops 49152 | bytes 198656 | tf_op jit(solution)/shard_map/mul | solution.py:870
  1.2 1.1 %fusion.2 = (f32[192,128]{1,0:T(8,128)}, f32[192,128]{1,0:T(8,128)}) fusion(f32[128]{0:T(128)S(1)} %get-tuple-element.11, f32[128]{0:T(128)S(1)} %get-tuple-element.12, f32[192]{0:T(256)S(1)} %add_convert_fusion.1, f32[128]{0:T(128)S(1)} %fusion.3), kind=kLoop, calls=%fused_computation.6 | loop fusion | flops 73728 | bytes 198912 | tf_op jit(solution)/shard_map/mul | solution.py:865
  2.3 105.2 %layer.1 = bf16[48,2048]{1,0:T(8,128)(2,1)} custom-call(bf16[192,512]{1,0:T(8,128)(2,1)} %latent_hbm.1, bf16[192,384]{1,0:T(8,128)(2,1)} %q_broad.1, bf16[192,256]{1,0:T(8,128)(2,1)} %q_narrow.1, f32[64,384]{1,0:T(8,128)} %get-tuple-element.6.cosines, f32[64,384]{1,0:T(8,128)} %get-tuple-element.5.sines, f32[192,128]{1,0:T(8,128)} %get-tuple-element.8.key_cosines, ...), custom_call_target="tpu_custom_call" | custom-call | flops 40000000000 | bytes 20000000 | tf_op jit(solution)/shard_map/layer/pallas_call | solution.py:768
  107.5 1.6 %copy.19 = bf16[48,2048]{1,0:T(8,128)(2,1)} copy(bf16[48,2048]{1,0:T(8,128)(2,1)} %layer.1) | data formatting | bytes 393216
  (5 shorter events, 0.0 us)
